TPU v7x, 32 devices: a whole 2x2x4 slice. The times are simulated.
32 devices in a mesh: sp: 8 (over z, x), tp: 4 (over y, core).
Axes of the slice: x: 2, y: 2, z: 4, core: 2. Of those that a mesh axis runs over, the one named last changes fastest.
Arguments:
- tokens: bfloat16 [6144, 4096], P('sp', 'tp'), may hold values from -6 to 6
- norm_gain: float32 [4096], replicated, may hold values from 0.1 to 1.9
- w_query: bfloat16 [4096, 2048], P('sp', 'tp'), may hold values from -0.09375 to 0.09375
- w_key: bfloat16 [4096, 1024], P('sp', 'tp'), may hold values from -0.09375 to 0.09375
- w_value: bfloat16 [4096, 1024], P('sp', 'tp'), may hold values from -0.09375 to 0.09375
- w_pool: bfloat16 [4096, 1024], P('sp', 'tp'), may hold values from -0.09375 to 0.09375
- query_gain: float32 [64], replicated, may hold values from 0.5 to 8
- key_gain: float32 [64], replicated, may hold values from 0.5 to 8
- sink_logit: float32 [32], P('tp'), may hold values from 1 to 5
- w_out_pool: bfloat16 [1024, 4096], P('tp', 'sp'), may hold values from -0.75 to 0.75
- w_out_attn: bfloat16 [2048, 4096], P('tp', 'sp'), may hold values from -1.5 to 1.5
Outputs:
- mixed: bfloat16 [6144, 4096], P(('sp', 'tp'))
All inputs are finite; a program needn't handle non-finite values.
Results may differ from a plain program's by a relative error of at most 0.014.
The roundings to bfloat16 on the way count: a program that leaves them out, or rounds other values in their place, can miss the bound.
Values may be sent and summed in bfloat16 or wider, within the bound.
A program may use at most 128 MiB of HBM per device.

v0:
```python
import functools

import jax
import jax.numpy as jnp
import numpy as np
from jax import lax
from jax.experimental import pallas as pl
from jax.experimental.pallas import tpu as pltpu
from jax.sharding import PartitionSpec as P

HEAD = 64
POOL = 1024
WINDOW = 128
GRID_W = 64

eps = 1e-06
rope_base = 10000.0
neg_big = -1e30
pool_pad = 16
chunks = 4
token_chunks = 8
MESH = pl.DeviceIdType.MESH
f32, bf16 = jnp.float32, jnp.bfloat16


def rope_parts(rows_total):
    quarter = HEAD // 4
    steps = np.arange(quarter, dtype=np.float32) * np.float32(2.0) / np.float32(HEAD // 2)
    freqs = (np.float32(1.0) / np.float32(rope_base) ** steps).astype(np.float32)

    def table(count, first):
        angle = np.arange(count, dtype=np.float32)[:, None] * freqs
        twice = np.concatenate([angle, angle], axis=1).astype(np.float64)
        none = np.zeros_like(twice)
        made = []
        for part in (np.cos(twice), np.sin(twice)):
            head = [part, none] if first else [none, part]
            made.append(np.concatenate(head + head, axis=1).astype(np.float32))
        return made

    return table(rows_total // GRID_W, True) + table(GRID_W, False)


def ring_place(index, count, across):
    deep = count // across
    if across == 1 or deep % 2:
        return index
    z, x = index // across, index % across
    turn = deep - 1 - z
    inner = jnp.where(turn % 2 == 0, x - 1, across - 1 - x)
    return jnp.where(x == 0, z, deep + turn * (across - 1) + inner)


def ring_index(place, count, across):
    deep = count // across
    if across == 1 or deep % 2:
        return place
    rest = jnp.maximum(place - deep, 0)
    turn, inner = rest // (across - 1), rest % (across - 1)
    x = jnp.where(turn % 2 == 0, inner + 1, across - 1 - inner)
    return jnp.where(place < deep, place * across, (deep - 1 - turn) * across + x)


def norm_rope(raw, gain, cosine, sine, low_half, lead):
    squares = raw * raw
    low_sum = jnp.sum(jnp.where(low_half, squares, 0.0), axis=1, keepdims=True)
    high_sum = jnp.sum(jnp.where(low_half, 0.0, squares), axis=1, keepdims=True)
    mean = jnp.where(low_half, low_sum, high_sum) * (1.0 / HEAD)
    scaled = raw * lax.rsqrt(mean + eps) * gain
    turned = jnp.where(
        lead,
        -pltpu.roll(scaled, 2 * HEAD - HEAD // 4, 1),
        pltpu.roll(scaled, HEAD // 4, 1),
    )
    return scaled * cosine + turned * sine


def layer_kernel(
    count,
    members,
    tokens,
    wq,
    wk,
    wv,
    wp,
    wop,
    woa,
    norm_gain,
    query_gain,
    key_gain,
    row_cos,
    row_sin,
    col_cos,
    col_sin,
    sink,
    out,
    tok,
    normed,
    w_side,
    w_query,
    w_out,
    side,
    query,
    band,
    pool_band,
    cosines,
    sines,
    mixer,
    away,
    met,
    kept,
    y_send,
    y_recv,
    done,
    load_sem,
    side_send,
    side_recv,
    query_send,
    query_recv,
    out_send,
    out_recv,
    ty_send,
    ty_recv,
    td_send,
    td_recv,
    halo_send,
    halo_recv,
    met_send,
    met_recv,
    yy_send,
    yy_recv,
    done_sem,
):
    rows, features = tokens.shape
    depth, kw = wk.shape
    qw, pw, width = wq.shape[1], wp.shape[1], wop.shape[1]
    chips = members // 2
    share = rows // members
    half = (count - 1) // 2
    heads_k = kw // HEAD
    seq = count * rows
    across = chips

    me, tp = lax.axis_index("sp"), lax.axis_index("tp")
    chip, core = tp // 2, tp % 2
    partner = chip * 2 + 1 - core
    place = ring_place(me, count, across)
    owner_of = lambda spot: ring_index(spot, count, across)
    at = lambda offset: (place + offset + count) % count
    following, previous = owner_of(at(1)), owner_of(at(-1))

    loads = [
        pltpu.make_async_copy(wk, w_side.at[place, :, pl.ds(0, kw)], load_sem.at[0]),
        pltpu.make_async_copy(wv, w_side.at[place, :, pl.ds(kw, kw)], load_sem.at[1]),
        pltpu.make_async_copy(wp, w_side.at[place, :, pl.ds(2 * kw, pw)], load_sem.at[2]),
        pltpu.make_async_copy(tokens, tok.at[tp], load_sem.at[3]),
        pltpu.make_async_copy(wq, w_query.at[place], load_sem.at[4]),
        pltpu.make_async_copy(wop, w_out.at[place, pl.ds(0, pw), :], load_sem.at[5]),
        pltpu.make_async_copy(woa, w_out.at[place, pl.ds(pw, qw), :], load_sem.at[6]),
    ]
    for load in loads:
        load.start()

    barrier = pltpu.get_barrier_semaphore()
    greeted = [
        (following, tp),
        (previous, tp),
        (me, partner),
        ((me + 1) % count, tp),
        ((me + count - 1) % count, tp),
    ]
    greeted += [(me, (chip + hop) % chips * 2 + core) for hop in range(1, chips)]
    for device in greeted:
        pl.semaphore_signal(barrier, inc=1, device_id=device, device_id_type=MESH)
    pl.semaphore_wait(barrier, len(greeted))

    def remote(source, target, send_sem, recv_sem, device):
        return pltpu.make_async_remote_copy(
            src_ref=source,
            dst_ref=target,
            send_sem=send_sem,
            recv_sem=recv_sem,
            device_id=device,
            device_id_type=MESH,
        )

    def hop_copy(ring, way, spot, c):
        buffer, send_sem, recv_sem = ring
        size = buffer.shape[1] // chunks
        part = buffer.at[spot, pl.ds(pl.multiple_of(c * size, 16), size), :]
        device = (following if way == 0 else previous, tp)
        return remote(part, part, send_sem.at[way, spot, c], recv_sem.at[spot, c], device)

    def send_own(ring):
        for c in range(chunks):
            hop_copy(ring, 0, place, c).start()
            hop_copy(ring, 1, place, c).start()

    def event(ring, step, c):
        low, high = at(-step), at(step)
        hop_copy(ring, 0, low, c).wait_recv()

        @pl.when((step < half) | (c < chunks // 2))
        def _():
            hop_copy(ring, 0, low, c).start()

        hop_copy(ring, 1, high, c).wait_recv()

        @pl.when((step < half) | (c >= chunks // 2))
        def _():
            hop_copy(ring, 1, high, c).start()

    def events(ring, step):
        def body(c, carry):
            event(ring, step, c)
            return carry

        lax.fori_loop(0, chunks, body, 0)

    def opposite(ring):
        def body(c, carry):
            hop_copy(ring, 0, at(count // 2), c).wait_recv()
            return carry

        lax.fori_loop(0, chunks, body, 0)

    def sends_done(ring):
        def each(c, carry):
            hop_copy(ring, 0, place, c).wait_send()
            hop_copy(ring, 1, place, c).wait_send()

            def steps(step, inner):
                @pl.when((step < half) | (c < chunks // 2))
                def _():
                    hop_copy(ring, 0, at(-step), c).wait_send()

                @pl.when((step < half) | (c >= chunks // 2))
                def _():
                    hop_copy(ring, 1, at(step), c).wait_send()

                return inner

            return lax.fori_loop(1, half + 1, steps, carry)

        lax.fori_loop(0, chunks, each, 0)

    side_ring = (w_side, side_send, side_recv)
    query_ring = (w_query, query_send, query_recv)
    out_ring = (w_out, out_send, out_recv)

    for load in loads[:3]:
        load.wait()
    send_own(side_ring)
    loads[3].wait()

    token_rows = rows // token_chunks

    def token_part(owner, j):
        return tok.at[owner, pl.ds(pl.multiple_of(j * token_rows, 16), token_rows), :]

    def token_far(hop, owner, j):
        part = token_part(owner, j)
        target = (chip + hop) % chips * 2 + core
        return remote(
            part, part, ty_send.at[hop - 1, j], ty_recv.at[hop - 1, j], (me, target)
        )

    def token_near(slot, owner, j):
        part = token_part(owner, j)
        return remote(part, part, td_send.at[slot, j], td_recv.at[slot, j], (me, partner))

    def start_tokens(j, carry):
        for hop in range(1, chips):
            token_far(hop, tp, j).start()
        token_near(0, tp, j).start()
        return carry

    lax.fori_loop(0, token_chunks, start_tokens, 0)

    for g in range(rows // GRID_W):
        spot = pl.ds(me * (rows // GRID_W) + g, 1)
        grid_rows = pl.ds(g * GRID_W, GRID_W)
        cosines[grid_rows, :] = col_cos[...] + row_cos[spot, :]
        sines[grid_rows, :] = col_sin[...] + row_sin[spot, :]

    pieces = features // depth
    norm_rows = 32 if token_rows % 32 == 0 else 16

    def normalise(j):
        token_near(0, partner, j).wait_recv()
        for hop in range(1, chips):
            token_near(hop, (chip - hop + chips) % chips * 2 + 1 - core, j).wait_recv()

        def tile(i, carry):
            at_rows = pl.ds(pl.multiple_of(j * token_rows + i * norm_rows, 16), norm_rows)
            squares = jnp.zeros((norm_rows, 1), f32)
            for t in range(members):
                block = tok[t, at_rows, :].astype(f32)
                squares = squares + jnp.sum(block * block, axis=1, keepdims=True)
            scale = lax.rsqrt(squares / (members * features) + eps)
            for t in range(members):
                for piece in range(pieces):
                    first = piece * depth
                    gain = norm_gain[:, t * features + first : t * features + first + depth]
                    block = tok[t, at_rows, first : first + depth].astype(f32)
                    normed[t * pieces + piece, at_rows, :] = (block * scale * gain).astype(bf16)
            return carry

        lax.fori_loop(0, token_rows // norm_rows, tile, 0)

    def token_step(j, carry):
        for hop in range(1, chips):
            source = (chip - hop + chips) % chips * 2 + core
            token_far(hop, source, j).wait_recv()
            token_near(hop, source, j).start()

        @pl.when(j < half * chunks)
        def _():
            event(side_ring, j // chunks + 1, j % chunks)

        @pl.when(j >= 1)
        def _():
            normalise(j - 1)

        return carry

    lax.fori_loop(0, token_chunks, token_step, 0)
    normalise(token_chunks - 1)

    tile_rows = 256 if rows % 256 == 0 else 128

    def project(total, weights, spots, first=False):
        def body(i, carry):
            part = pl.ds(pl.multiple_of(i * tile_rows, tile_rows), tile_rows)
            terms = [
                jnp.dot(
                    normed[owner_of(spot), part, :], weights[spot], preferred_element_type=f32
                )
                for spot in spots
            ]
            value = functools.reduce(lambda a, b: a + b, terms)
            total[part, :] = value if first else total[part, :] + value
            return carry

        lax.fori_loop(0, rows // tile_rows, body, 0)

    project(side, w_side, [place], first=True)
    early = token_chunks // chunks

    def side_step(step, carry):
        @pl.when(step > early)
        def _():
            events(side_ring, step)

        project(side, w_side, [at(-step), at(step)])
        return carry

    lax.fori_loop(1, half + 1, side_step, 0)
    loads[4].wait()
    send_own(query_ring)
    opposite(side_ring)
    project(side, w_side, [at(count // 2)])

    lane = lax.broadcasted_iota(jnp.int32, (WINDOW, 2 * HEAD), 1)
    low_half = lane < HEAD
    lead = lane % (HEAD // 2) < HEAD // 4

    def prepare(i, carry):
        part = pl.ds(pl.multiple_of(i * WINDOW, WINDOW), WINDOW)
        shifted = pl.ds(pl.multiple_of((i + 1) * WINDOW, WINDOW), WINDOW)
        for h in range(kw // (2 * HEAD)):
            lanes = slice(h * 2 * HEAD, (h + 1) * 2 * HEAD)
            key = norm_rope(
                side[part, lanes], key_gain[...], cosines[part, :], sines[part, :], low_half, lead
            )
            band[shifted, lanes] = key.astype(bf16)
        band[shifted, kw : 2 * kw] = side[part, kw : 2 * kw].astype(bf16)
        pooled_rows = pl.ds(pl.multiple_of(i * WINDOW + pool_pad, pool_pad), WINDOW)
        pool_band[pooled_rows, :] = side[part, 2 * kw :].astype(bf16)
        return carry

    lax.fori_loop(0, rows // WINDOW, prepare, 0)

    before, behind = (me + count - 1) % count, (me + 1) % count

    def halo(index, buffer, size, upwards):
        if upwards:
            source, target, device = rows, 0, (behind, tp)
        else:
            source, target, device = size, rows + size, (before, tp)
        return remote(
            buffer.at[pl.ds(source, size), :],
            buffer.at[pl.ds(target, size), :],
            halo_send.at[index],
            halo_recv.at[index],
            device,
        )

    lower = [halo(0, band, WINDOW, False), halo(1, pool_band, pool_pad, False)]
    upper = [halo(2, band, WINDOW, True), halo(3, pool_band, pool_pad, True)]
    has_lower, has_upper = me > 0, me < count - 1

    @pl.when(has_lower)
    def _():
        for copy in lower:
            copy.start()

    @pl.when(has_upper)
    def _():
        for copy in upper:
            copy.start()

    @pl.when(jnp.logical_not(has_lower))
    def _():
        band[0:WINDOW, :] = jnp.zeros((WINDOW, 2 * kw), bf16)
        pool_band[0:pool_pad, :] = jnp.zeros((pool_pad, pw), bf16)

    @pl.when(jnp.logical_not(has_upper))
    def _():
        band[rows + WINDOW :, :] = jnp.zeros((WINDOW, 2 * kw), bf16)
        pool_band[rows + pool_pad :, :] = jnp.zeros((pool_pad, pw), bf16)

    project(query, w_query, [place], first=True)

    def query_step(step, carry):
        events(query_ring, step)
        project(query, w_query, [at(-step), at(step)])
        return carry

    lax.fori_loop(1, half + 1, query_step, 0)
    loads[5].wait()
    loads[6].wait()
    send_own(out_ring)

    @pl.when(has_lower)
    def _():
        for copy in upper:
            copy.wait_recv()

    @pl.when(has_upper)
    def _():
        for copy in lower:
            copy.wait_recv()

    level = tp * pw // (POOL // 4)
    reach = jnp.where(level == 0, 1, jnp.where(level == 1, 2, jnp.where(level == 2, 4, 8)))

    def pool(i, carry):
        wide = WINDOW + 2 * pool_pad
        part = pl.ds(pl.multiple_of(i * WINDOW, WINDOW), WINDOW)
        values = pool_band[pl.ds(pl.multiple_of(i * WINDOW, pool_pad), wide), :].astype(f32)
        total, chosen = values, None
        for step in range(4):
            size = 2**step
            total = total + pltpu.roll(total, wide - size, 0)
            shifted = pltpu.roll(total, size, 0)[pool_pad : pool_pad + WINDOW]
            chosen = shifted if chosen is None else jnp.where(level == step, shifted, chosen)
        spot = me * rows + i * WINDOW + lax.broadcasted_iota(jnp.int32, (WINDOW, 1), 0)
        low = jnp.maximum(spot - reach, 0)
        high = jnp.minimum(spot + reach - 1, seq - 1)
        mixer[part, 0:pw] = (chosen / (high - low + 1).astype(f32)).astype(bf16)
        return carry

    lax.fori_loop(0, rows // WINDOW, pool, 0)

    opposite(query_ring)
    project(query, w_query, [at(count // 2)])

    blocks = rows // WINDOW
    row = lax.broadcasted_iota(jnp.int32, (2 * WINDOW, 3 * WINDOW), 0) % WINDOW
    column = lax.broadcasted_iota(jnp.int32, (2 * WINDOW, 3 * WINDOW), 1)
    top_row = lax.broadcasted_iota(jnp.int32, (2 * WINDOW, 1), 0) < WINDOW

    def attend(i, carry):
        part = pl.ds(pl.multiple_of(i * WINDOW, WINDOW), WINDOW)
        key_rows = pl.ds(pl.multiple_of(i * WINDOW, WINDOW), 3 * WINDOW)
        key_pos = me * rows + i * WINDOW - WINDOW + column
        inside = (column >= row) & (column - row <= 2 * WINDOW) & (key_pos >= 0) & (key_pos < seq)
        for head in range(heads_k):
            lanes = slice(head * 2 * HEAD, (head + 1) * 2 * HEAD)
            rotated = norm_rope(
                query[part, lanes],
                query_gain[...],
                cosines[part, :],
                sines[part, :],
                low_half,
                lead,
            ) * HEAD ** (-0.5)
            other = pltpu.roll(rotated, HEAD, 1)
            if head % 2 == 0:
                pair = (jnp.where(low_half, rotated, 0.0), jnp.where(low_half, other, 0.0))
            else:
                pair = (jnp.where(low_half, 0.0, other), jnp.where(low_half, 0.0, rotated))
            stacked = jnp.concatenate(pair, axis=0).astype(bf16)
            tile = head // 2 * 2 * HEAD
            keys = band[key_rows, tile : tile + 2 * HEAD]
            values = band[key_rows, kw + tile : kw + tile + 2 * HEAD]
            scores = lax.dot_general(
                stacked, keys, (((1,), (1,)), ((), ())), preferred_element_type=f32
            )
            scores = jnp.where(inside, scores, neg_big)
            limit = jnp.where(top_row, sink[2 * head], sink[2 * head + 1])
            top = jnp.maximum(jnp.max(scores, axis=1, keepdims=True), limit)
            raised = jnp.exp(scores - top)
            totals = jnp.sum(raised, axis=1, keepdims=True) + jnp.exp(limit - top)
            weights = (raised * (1.0 / totals)).astype(bf16)
            result = jnp.dot(weights, values, preferred_element_type=f32)
            one, two = result[:WINDOW], result[WINDOW:]
            if head % 2 == 0:
                joined = jnp.where(low_half, one, pltpu.roll(two, HEAD, 1))
            else:
                joined = jnp.where(low_half, pltpu.roll(one, HEAD, 1), two)
            mixer[part, pw + head * 2 * HEAD : pw + (head + 1) * 2 * HEAD] = joined.astype(bf16)

        for c in range(chunks):

            @pl.when(i == ((c + 1) * blocks + chunks - 1) // chunks - 1)
            def _(c=c):
                event(out_ring, 1, c)

        return carry

    lax.fori_loop(0, blocks, attend, 0)

    def product(spot, which):
        left = jnp.concatenate(
            [
                mixer[pl.ds(pl.multiple_of((y * 2 + which) * share, 16), share), :]
                for y in range(chips)
            ],
            axis=0,
        )
        return jnp.dot(left, w_out[spot], preferred_element_type=f32).astype(bf16)

    def met_copy(spot):
        return remote(
            away.at[spot], met.at[spot], met_send.at[spot], met_recv.at[spot], (me, partner)
        )

    def y_copy(spot, hop):
        target = (chip + hop) % chips * 2 + core
        return remote(
            y_send.at[spot, hop - 1],
            y_recv.at[spot, hop - 1],
            yy_send.at[spot, hop - 1],
            yy_recv.at[spot, hop - 1],
            (me, target),
        )

    def done_copy(spot):
        columns = pl.ds(pl.multiple_of(owner_of(spot) * width, width), width)
        return pltpu.make_async_copy(done.at[spot], out.at[:, columns], done_sem.at[spot])

    def both_rows(spot, y):
        part = pl.ds(pl.multiple_of(y * share, 16), share)
        return kept[spot, part, :].astype(f32) + met[spot, part, :].astype(f32)

    def group(spots):
        def first(spot):
            away[spot] = product(spot, 1 - core)
            met_copy(spot).start()

        def second(spot):
            kept[spot] = product(spot, core)

        def third(spot):
            met_copy(spot).wait_recv()
            for hop in range(1, chips):
                y_send[spot, hop - 1] = both_rows(spot, (chip + hop) % chips).astype(bf16)
                y_copy(spot, hop).start()

        for part in (first, second, third):
            for spot in spots:
                part(spot)

    def finish(spot):
        total = both_rows(spot, chip)
        for hop in range(1, chips):
            y_copy(spot, hop).wait_recv()
            total = total + y_recv[spot, hop - 1].astype(f32)
        done[spot] = total.astype(bf16)
        done_copy(spot).start()

    group([place])

    def out_step(step, carry):
        @pl.when(step > 1)
        def _():
            events(out_ring, step)

        group([at(-step), at(step)])

        @pl.when(step == 1)
        def _():
            finish(place)

        @pl.when(step > 1)
        def _():
            finish(at(1 - step))
            finish(at(step - 1))

        return carry

    lax.fori_loop(1, half + 1, out_step, 0)
    opposite(out_ring)
    group([at(count // 2)])
    finish(at(-half))
    finish(at(half))
    finish(at(count // 2))

    for ring in (side_ring, query_ring, out_ring):
        sends_done(ring)

    def tokens_sent(j, carry):
        token_near(0, tp, j).wait_send()
        for hop in range(1, chips):
            token_far(hop, tp, j).wait_send()
            token_near(hop, (chip - hop + chips) % chips * 2 + core, j).wait_send()
        return carry

    lax.fori_loop(0, token_chunks, tokens_sent, 0)

    @pl.when(has_lower)
    def _():
        for copy in lower:
            copy.wait_send()

    @pl.when(has_upper)
    def _():
        for copy in upper:
            copy.wait_send()

    def blocks_sent(spot, carry):
        met_copy(spot).wait_send()
        for hop in range(1, chips):
            y_copy(spot, hop).wait_send()
        done_copy(spot).wait()
        return carry

    lax.fori_loop(0, count, blocks_sent, 0)


def shards(
    tokens,
    norm_gain,
    w_query,
    w_key,
    w_value,
    w_pool,
    query_gain,
    key_gain,
    sink_logit,
    w_out_pool,
    w_out_attn,
):
    count, members = lax.axis_size("sp"), lax.axis_size("tp")
    rows, features = tokens.shape
    depth, kw = w_key.shape
    qw, pw, width = w_query.shape[1], w_pool.shape[1], w_out_pool.shape[1]
    chips, share = members // 2, rows // members
    tables = [jnp.asarray(table) for table in rope_parts(count * rows)]
    twice = lambda gain: jnp.concatenate([gain, gain]).reshape(1, 2 * HEAD)
    anywhere = pl.BlockSpec(memory_space=pl.ANY)
    in_vmem = pl.BlockSpec(memory_space=pltpu.VMEM)
    dma = pltpu.SemaphoreType.DMA
    far = max(chips - 1, 1)
    return pl.pallas_call(
        functools.partial(layer_kernel, count, members),
        out_shape=jax.ShapeDtypeStruct((share, count * width), bf16),
        in_specs=[anywhere] * 7 + [in_vmem] * 7 + [pl.BlockSpec(memory_space=pltpu.SMEM)],
        out_specs=anywhere,
        scratch_shapes=[
            pltpu.VMEM((members, rows, features), bf16),
            pltpu.VMEM((count, rows, depth), bf16),
            pltpu.VMEM((count, depth, 2 * kw + pw), bf16),
            pltpu.VMEM((count, depth, qw), bf16),
            pltpu.VMEM((count, pw + qw, width), bf16),
            pltpu.VMEM((rows, 2 * kw + pw), f32),
            pltpu.VMEM((rows, qw), f32),
            pltpu.VMEM((rows + 2 * WINDOW, 2 * kw), bf16),
            pltpu.VMEM((rows + 2 * pool_pad, pw), bf16),
            pltpu.VMEM((rows, 2 * HEAD), f32),
            pltpu.VMEM((rows, 2 * HEAD), f32),
            pltpu.VMEM((rows, pw + qw), bf16),
            pltpu.VMEM((count, chips * share, width), bf16),
            pltpu.VMEM((count, chips * share, width), bf16),
            pltpu.VMEM((count, chips * share, width), bf16),
            pltpu.VMEM((count, far, share, width), bf16),
            pltpu.VMEM((count, far, share, width), bf16),
            pltpu.VMEM((count, share, width), bf16),
            dma((7,)),
            dma((2, count, chunks)),
            dma((count, chunks)),
            dma((2, count, chunks)),
            dma((count, chunks)),
            dma((2, count, chunks)),
            dma((count, chunks)),
            dma((far, token_chunks)),
            dma((far, token_chunks)),
            dma((chips, token_chunks)),
            dma((chips, token_chunks)),
            dma((4,)),
            dma((4,)),
            dma((count,)),
            dma((count,)),
            dma((count, far)),
            dma((count, far)),
            dma((count,)),
        ],
        compiler_params=pltpu.CompilerParams(
            collective_id=0, has_side_effects=True, vmem_limit_bytes=60 * 1024 * 1024
        ),
    )(
        tokens,
        w_query,
        w_key,
        w_value,
        w_pool,
        w_out_pool,
        w_out_attn,
        norm_gain.reshape(1, -1),
        twice(query_gain),
        twice(key_gain),
        *tables,
        sink_logit,
    )


def solution(mesh):
    placed = (
        P("sp", "tp"),
        P(),
        P("sp", "tp"),
        P("sp", "tp"),
        P("sp", "tp"),
        P("sp", "tp"),
        P(),
        P(),
        P("tp"),
        P("tp", "sp"),
        P("tp", "sp"),
    )
    return jax.shard_map(
        shards, mesh=mesh, in_specs=placed, out_specs=P(("sp", "tp"), None), check_vma=False
    )
```

profile of v0, /device:TPU:1, one launch (start us, length us, event | category | flops | bytes accessed | tf_op | source)
XLA Modules:
  0.0 187.6 jit_solution(13738837323628740459)
XLA Ops:
  0.0 1.4 maximum_bitcast_fusion
  1.4 183.5 %shard_map.145 = bf16[192,4096]{1,0:T(8,128)(2,1)} custom-call(bf16[768,1024]{1,0:T(8,128)(2,1)} %tokens.1, bf16[512,512]{1,0:T(8,128)(2,1)} %wq.1, bf16[512,256]{1,0:T(8,128)(2,1)} %wk.1, bf16[512,256]{1,0:T(8,128)(2,1)} %wv.1, bf16[512,256]{1,0:T(8,128)(2,1)} %wp.1, bf16[256,512]{1,0:T(8,128)(2,1)} %wop.1, bf16[512,512]{1,0:T(8,128)(2,1)} %woa.1, ...), custom_call_target="tpu_custom_call" | custom-call | tf_op jit(solution)/shard_map/pallas_call | solution.py:667
  184.9 2.7 %copy.17 = bf16[192,4096]{1,0:T(8,128)(2,1)} copy(bf16[192,4096]{1,0:T(8,128)(2,1)} %shard_map.145) | data formatting | bytes 3145728
where the time goes:
time: 189 us; the launch traced here: 188 us
  Pallas kernels  183 us (97%)
  local copies, waits for them, and re-layouts  2.7 us (1%)
    pallas_call x1, Pallas kernels, shards(): pl.pallas_call(functools.partial(layer_kernel, count, members), out_shape...  183 us

commit v1 on v0

--- a/solution.py
+++ b/solution.py
@@ -19,6 +19,8 @@
 pool_pad = 16
 chunks = 4
 token_chunks = 8
+in_parts = 4
+out_parts = 2
 MESH = pl.DeviceIdType.MESH
 f32, bf16 = jnp.float32, jnp.bfloat16
 
@@ -640,6 +642,833 @@
     lax.fori_loop(0, count, blocks_sent, 0)
 
 
+def plane_kernel(
+    count,
+    members,
+    tokens,
+    wq,
+    wk,
+    wv,
+    wp,
+    wop,
+    woa,
+    norm_gain,
+    query_gain,
+    key_gain,
+    row_cos,
+    row_sin,
+    col_cos,
+    col_sin,
+    sink,
+    out,
+    raw,
+    sums,
+    normed,
+    w_in,
+    w_pool,
+    w_out,
+    in_spare,
+    pool_spare,
+    out_spare,
+    total,
+    pool_total,
+    band,
+    pool_band,
+    cosines,
+    sines,
+    mixer,
+    away,
+    met,
+    kept,
+    one_send,
+    one_recv,
+    two_send,
+    two_recv,
+    done,
+    load_sem,
+    sum_send,
+    sum_recv,
+    in_sems,
+    pool_sems,
+    out_sems,
+    x_sems,
+    tx_send,
+    tx_recv,
+    ty_send,
+    ty_recv,
+    td_send,
+    td_recv,
+    halo_send,
+    halo_recv,
+    met_send,
+    met_recv,
+    hop_send,
+    hop_recv,
+    done_sem,
+):
+    rows, features = tokens.shape
+    depth = wk.shape[0]
+    hk, hq, hp = wk.shape[1] // 2, wq.shape[1] // 2, wp.shape[1] // 2
+    width = wop.shape[1]
+    narrow = width // out_parts
+    share = rows // members
+    plane = 2 * rows
+    heads_k = hk // HEAD
+    seq = count * rows
+    deep = count // 2
+    pieces = features // depth
+    tiles = rows // WINDOW
+
+    me, tp = lax.axis_index("sp"), lax.axis_index("tp")
+    z, x = me // 2, me % 2
+    y, core = tp // 2, tp % 2
+    me_x, tp_y, tp_c = me + 1 - 2 * x, (1 - y) * 2 + core, y * 2 + 1 - core
+    tp_yc = (1 - y) * 2 + 1 - core
+    up, down = (me + 2) % count, (me + count - 2) % count
+    has_up, has_down = z < deep - 1, z > 0
+    inner = has_up & has_down
+
+    mine = lambda size: pl.ds(pl.multiple_of(x * size, 128), size)
+    other = lambda size: pl.ds(pl.multiple_of((1 - x) * size, 128), size)
+    loads = []
+
+    def load(source, target):
+        loads.append(pltpu.make_async_copy(source, target, load_sem.at[len(loads)]))
+        loads[-1].start()
+
+    for target, pick in ((w_in.at[me], mine), (in_spare, other)):
+        load(wk.at[:, pick(hk)], target.at[:, pl.ds(0, hk)])
+        load(wv.at[:, pick(hk)], target.at[:, pl.ds(hk, hk)])
+        load(wq.at[:, pick(hq)], target.at[:, pl.ds(2 * hk, hq)])
+    load(tokens, raw)
+    for target, pick in ((w_pool.at[me], mine), (pool_spare, other)):
+        load(wp.at[:, pick(hp)], target)
+    for target, pick in ((w_out.at[me], mine), (out_spare, other)):
+        for part in range(out_parts):
+            columns = pl.ds(part * narrow, narrow)
+            load(wop.at[pick(hp), columns], target.at[part, pl.ds(0, hp), :])
+            load(woa.at[pick(hq), columns], target.at[part, pl.ds(hp, hq), :])
+
+    barrier = pltpu.get_barrier_semaphore()
+    greeted = [(up, tp), (down, tp), (me_x, tp), (me, tp_y), (me, tp_c), (me, tp_yc)]
+    for device in greeted:
+        pl.semaphore_signal(barrier, inc=1, device_id=device, device_id_type=MESH)
+    pl.semaphore_wait(barrier, len(greeted))
+
+    def remote(source, target, send_sem, recv_sem, device):
+        return pltpu.make_async_remote_copy(
+            src_ref=source,
+            dst_ref=target,
+            send_sem=send_sem,
+            recv_sem=recv_sem,
+            device_id=device,
+            device_id_type=MESH,
+        )
+
+    def by_rows(parts):
+        def view(buffer, c):
+            size = buffer.shape[0] // parts
+            return buffer.at[pl.ds(pl.multiple_of(c * size, 16), size), :]
+
+        return view
+
+    in_ring = (w_in, in_spare, in_sems, 0, in_parts, by_rows(in_parts), True)
+    pool_ring = (w_pool, pool_spare, pool_sems, in_parts, 1, by_rows(1), False)
+    out_ring = (
+        w_out,
+        out_spare,
+        out_sems,
+        in_parts + 1,
+        out_parts,
+        lambda buffer, c: buffer.at[c],
+        False,
+    )
+
+    def z_copy(ring, way, source, c):
+        buffer, _, sems, _, _, view, _ = ring
+        part = view(buffer.at[source], c)
+        return remote(
+            part, part, sems.at[way, source, c], sems.at[2, source, c], ((up, down)[way], tp)
+        )
+
+    def x_copy(ring, source, c):
+        buffer, spare, sems, first, _, view, _ = ring
+        return remote(
+            view(spare, c),
+            view(buffer.at[source], c),
+            x_sems.at[first + c],
+            sems.at[2, source, c],
+            (me_x, tp),
+        )
+
+    def both_ways(ring, source, c, act):
+        @pl.when(has_up)
+        def _():
+            act(z_copy(ring, 0, source, c))
+
+        @pl.when(has_down)
+        def _():
+            act(z_copy(ring, 1, source, c))
+
+    start = lambda copy: copy.start()
+    sent = lambda copy: copy.wait_send()
+
+    def own_out(ring):
+        for c in range(ring[4]):
+            both_ways(ring, me, c, start)
+
+    def side_out(ring):
+        for c in range(ring[4]):
+            x_copy(ring, me, c).start()
+
+    def side_in(ring):
+        for c in range(ring[4]):
+            x_copy(ring, me_x, c).wait_recv()
+            both_ways(ring, me_x, c, start)
+
+    def passing(ring, n):
+        parts = ring[4]
+        step, j, c = n // (2 * parts) + 1, n // parts % 2, n % parts
+        column = (x + j) % 2 if ring[6] else j
+        low, high = z - step, z + step
+        return (low >= 0, low * 2 + column), (high < deep, high * 2 + column), c
+
+    def event(ring, n):
+        (is_low, low), (is_high, high), c = passing(ring, n)
+
+        @pl.when(is_low)
+        def _():
+            z_copy(ring, 0, low, c).wait_recv()
+
+            @pl.when(has_up)
+            def _():
+                z_copy(ring, 0, low, c).start()
+
+        @pl.when(is_high)
+        def _():
+            z_copy(ring, 1, high, c).wait_recv()
+
+            @pl.when(has_down)
+            def _():
+                z_copy(ring, 1, high, c).start()
+
+    def events(ring, first, last):
+        def body(n, carry):
+            event(ring, n)
+            return carry
+
+        lax.fori_loop(first, last, body, 0)
+
+    def all_events(ring):
+        return (deep - 1) * 2 * ring[4]
+
+    def sends_done(ring):
+        for c in range(ring[4]):
+            both_ways(ring, me, c, sent)
+            both_ways(ring, me_x, c, sent)
+            x_copy(ring, me, c).wait_send()
+
+        def body(n, carry):
+            (is_low, low), (is_high, high), c = passing(ring, n)
+
+            @pl.when(is_low & has_up)
+            def _():
+                z_copy(ring, 0, low, c).wait_send()
+
+            @pl.when(is_high & has_down)
+            def _():
+                z_copy(ring, 1, high, c).wait_send()
+
+            return carry
+
+        lax.fori_loop(0, all_events(ring), body, 0)
+
+    for copy in loads[:6]:
+        copy.wait()
+    for c in range(in_parts):
+        x_copy(in_ring, me, c).start()
+        both_ways(in_ring, me, c, start)
+
+    loads[6].wait()
+    sums[tp] = jnp.zeros_like(sums[tp])
+    for i in range(tiles):
+        block = raw[i * WINDOW : (i + 1) * WINDOW, :].astype(f32)
+        square = jnp.sum(block * block, axis=1, keepdims=True)
+        turned = jnp.transpose(jnp.broadcast_to(square, (WINDOW, WINDOW)))
+        sums[tp, i : i + 1, :] = turned[0:1, :]
+
+    def sum_copy(owner, hop):
+        target = (tp + hop) % members
+        return remote(
+            sums.at[owner],
+            sums.at[owner],
+            sum_send.at[hop - 1],
+            sum_recv.at[hop - 1],
+            (me, target),
+        )
+
+    for hop in range(1, members):
+        sum_copy(tp, hop).start()
+    for g in range(plane // GRID_W):
+        spot = pl.ds(z * (plane // GRID_W) + g, 1)
+        grid_rows = pl.ds(g * GRID_W, GRID_W)
+        cosines[grid_rows, :] = col_cos[...] + row_cos[spot, :]
+        sines[grid_rows, :] = col_sin[...] + row_sin[spot, :]
+    for hop in range(1, members):
+        sum_copy((tp - hop + members) % members, hop).wait_recv()
+    squares = sums[0]
+    for t in range(1, members):
+        squares = squares + sums[t]
+    scales = lax.rsqrt(squares / (members * features) + eps)
+
+    def token_part(side, owner, j):
+        return normed.at[
+            side,
+            pl.ds(owner * pieces, pieces),
+            pl.ds(pl.multiple_of(j * WINDOW, WINDOW), WINDOW),
+            :,
+        ]
+
+    def over_x(slot, side, owner, j):
+        part = token_part(side, owner, j)
+        return remote(part, part, tx_send.at[slot, j], tx_recv.at[slot, j], (me_x, tp))
+
+    def over_y(slot, side, owner, j):
+        part = token_part(side, owner, j)
+        return remote(part, part, ty_send.at[slot, j], ty_recv.at[slot, j], (me, tp_y))
+
+    def over_core(slot, side, owner, j):
+        part = token_part(side, owner, j)
+        return remote(part, part, td_send.at[slot, j], td_recv.at[slot, j], (me, tp_c))
+
+    gains = norm_gain[pl.ds(tp, 1), :]
+    for i in range(tiles):
+        here = slice(i * WINDOW, (i + 1) * WINDOW)
+        scale = jnp.transpose(jnp.broadcast_to(scales[i : i + 1, :], (WINDOW, WINDOW)))
+        for first in range(0, features, WINDOW):
+            block = raw[here, first : first + WINDOW].astype(f32)
+            value = (block * scale * gains[:, first : first + WINDOW]).astype(bf16)
+            inside = first % depth
+            normed[x, tp * pieces + first // depth, here, inside : inside + WINDOW] = value
+        over_y(0, x, tp, i).start()
+        over_x(0, x, tp, i).start()
+        over_core(0, x, tp, i).start()
+
+    side_in(in_ring)
+    whole = all_events(in_ring)
+    reached = lambda part: whole * part // 24
+    events(in_ring, 0, reached(4))
+
+    def by_x(j):
+        return j % 3 == 0
+
+    def direct(j, carry):
+        over_y(0, x, tp_y, j).wait_recv()
+        over_core(2, x, tp_y, j).start()
+
+        @pl.when(by_x(j))
+        def _():
+            over_x(1, x, tp_y, j).start()
+
+        over_x(0, 1 - x, tp, j).wait_recv()
+        over_core(1, 1 - x, tp, j).start()
+
+        @pl.when(jnp.logical_not(by_x(j)))
+        def _():
+            over_y(1, 1 - x, tp, j).start()
+
+        events(in_ring, reached(4 + 12 * j // tiles), reached(4 + 12 * (j + 1) // tiles))
+        return carry
+
+    lax.fori_loop(0, tiles, direct, 0)
+    for copy in loads[7:]:
+        copy.wait()
+    side_out(pool_ring)
+    side_out(out_ring)
+
+    def crossed(j, carry):
+        @pl.when(by_x(j))
+        def _():
+            over_x(1, 1 - x, tp_y, j).wait_recv()
+
+        @pl.when(jnp.logical_not(by_x(j)))
+        def _():
+            over_y(1, 1 - x, tp_y, j).wait_recv()
+
+        over_core(3, 1 - x, tp_y, j).start()
+        events(in_ring, reached(16 + 6 * j // tiles), reached(16 + 6 * (j + 1) // tiles))
+        return carry
+
+    lax.fori_loop(0, tiles, crossed, 0)
+    own_out(pool_ring)
+
+    def from_core(j, carry):
+        over_core(0, x, tp_c, j).wait_recv()
+        over_core(1, 1 - x, tp_c, j).wait_recv()
+        over_core(2, x, tp_yc, j).wait_recv()
+        over_core(3, 1 - x, tp_yc, j).wait_recv()
+        return carry
+
+    lax.fori_loop(0, tiles, from_core, 0)
+
+    tile_rows = 256 if rows % 256 == 0 else 128
+    per_side = rows // tile_rows
+
+    def project(result, weights, level, first=False):
+        def body(i, carry):
+            part = pl.ds(pl.multiple_of(i * tile_rows, tile_rows), tile_rows)
+            within = pl.ds(pl.multiple_of(i % per_side * tile_rows, tile_rows), tile_rows)
+            value = None if first else result[part, :]
+            for j in range(2):
+                term = jnp.dot(
+                    normed[i // per_side, level * 2 + j, within, :],
+                    weights[level * 2 + j],
+                    preferred_element_type=f32,
+                )
+                value = term if value is None else value + term
+            result[part, :] = value
+            return carry
+
+        lax.fori_loop(0, 2 * per_side, body, 0)
+
+    def project_step(result, weights, step):
+        @pl.when(z - step >= 0)
+        def _():
+            project(result, weights, z - step)
+
+        @pl.when(z + step < deep)
+        def _():
+            project(result, weights, z + step)
+
+    project(total, w_in, z, first=True)
+
+    def in_step(step, carry):
+        each = 2 * in_parts
+        events(in_ring, jnp.maximum((step - 1) * each, reached(22)), step * each)
+        project_step(total, w_in, step)
+        return carry
+
+    lax.fori_loop(1, deep, in_step, 0)
+
+    lane = lax.broadcasted_iota(jnp.int32, (WINDOW, 2 * HEAD), 1)
+    low_half = lane < HEAD
+    lead = lane % (HEAD // 2) < HEAD // 4
+    blocks = plane // WINDOW
+
+    def prepare(i, carry):
+        part = pl.ds(pl.multiple_of(i * WINDOW, WINDOW), WINDOW)
+        shifted = pl.ds(pl.multiple_of((i + 1) * WINDOW, WINDOW), WINDOW)
+        for h in range(hk // (2 * HEAD)):
+            lanes = slice(h * 2 * HEAD, (h + 1) * 2 * HEAD)
+            key = norm_rope(
+                total[part, lanes], key_gain[...], cosines[part, :], sines[part, :], low_half, lead
+            )
+            band[shifted, lanes] = key.astype(bf16)
+        band[shifted, hk:] = total[part, hk : 2 * hk].astype(bf16)
+        return carry
+
+    lax.fori_loop(0, blocks, prepare, 0)
+
+    def halo(index, buffer, size, upwards):
+        if upwards:
+            source, target, device = plane, 0, (up, tp)
+        else:
+            source, target, device = size, plane + size, (down, tp)
+        return remote(
+            buffer.at[pl.ds(source, size), :],
+            buffer.at[pl.ds(target, size), :],
+            halo_send.at[index],
+            halo_recv.at[index],
+            device,
+        )
+
+    def halo_out(index, buffer, size):
+        @pl.when(has_down)
+        def _():
+            halo(index, buffer, size, False).start()
+
+        @pl.when(has_up)
+        def _():
+            halo(index + 1, buffer, size, True).start()
+
+        empty = jnp.zeros((size, buffer.shape[1]), bf16)
+
+        @pl.when(jnp.logical_not(has_down))
+        def _():
+            buffer[0:size, :] = empty
+
+        @pl.when(jnp.logical_not(has_up))
+        def _():
+            buffer[plane + size :, :] = empty
+
+    def halo_in(index, buffer, size):
+        @pl.when(has_up)
+        def _():
+            halo(index, buffer, size, False).wait_recv()
+
+        @pl.when(has_down)
+        def _():
+            halo(index + 1, buffer, size, True).wait_recv()
+
+    halo_out(0, band, WINDOW)
+
+    def pool_stage():
+        side_in(pool_ring)
+        project(pool_total, w_pool, z, first=True)
+
+        def step_body(step, carry):
+            events(pool_ring, (step - 1) * 2, step * 2)
+            project_step(pool_total, w_pool, step)
+            return carry
+
+        lax.fori_loop(1, deep, step_body, 0)
+        pool_band[pool_pad : pool_pad + plane, :] = pool_total[...].astype(bf16)
+        halo_out(2, pool_band, pool_pad)
+
+    @pl.when(inner)
+    def _():
+        pool_stage()
+
+    own_out(out_ring)
+    side_in(out_ring)
+
+    row = lax.broadcasted_iota(jnp.int32, (2 * WINDOW, 3 * WINDOW), 0) % WINDOW
+    column = lax.broadcasted_iota(jnp.int32, (2 * WINDOW, 3 * WINDOW), 1)
+    top_row = lax.broadcasted_iota(jnp.int32, (2 * WINDOW, 1), 0) < WINDOW
+
+    def attend(turn, carry):
+        @pl.when(turn == blocks - 2)
+        def _():
+            halo_in(0, band, WINDOW)
+
+        i = (turn + 1) % blocks
+        part = pl.ds(pl.multiple_of(i * WINDOW, WINDOW), WINDOW)
+        key_rows = pl.ds(pl.multiple_of(i * WINDOW, WINDOW), 3 * WINDOW)
+        key_pos = z * plane + i * WINDOW - WINDOW + column
+        inside = (column >= row) & (column - row <= 2 * WINDOW) & (key_pos >= 0) & (key_pos < seq)
+        for head in range(heads_k):
+            lanes = slice(2 * hk + head * 2 * HEAD, 2 * hk + (head + 1) * 2 * HEAD)
+            rotated = norm_rope(
+                total[part, lanes],
+                query_gain[...],
+                cosines[part, :],
+                sines[part, :],
+                low_half,
+                lead,
+            ) * HEAD ** (-0.5)
+            swapped = pltpu.roll(rotated, HEAD, 1)
+            if head % 2 == 0:
+                pair = (jnp.where(low_half, rotated, 0.0), jnp.where(low_half, swapped, 0.0))
+            else:
+                pair = (jnp.where(low_half, 0.0, swapped), jnp.where(low_half, 0.0, rotated))
+            stacked = jnp.concatenate(pair, axis=0).astype(bf16)
+            tile = head // 2 * 2 * HEAD
+            keys = band[key_rows, tile : tile + 2 * HEAD]
+            values = band[key_rows, hk + tile : hk + tile + 2 * HEAD]
+            scores = lax.dot_general(
+                stacked, keys, (((1,), (1,)), ((), ())), preferred_element_type=f32
+            )
+            scores = jnp.where(inside, scores, neg_big)
+            first = x * 2 * heads_k + 2 * head
+            limit = jnp.where(top_row, sink[first], sink[first + 1])
+            top = jnp.maximum(jnp.max(scores, axis=1, keepdims=True), limit)
+            raised = jnp.exp(scores - top)
+            totals = jnp.sum(raised, axis=1, keepdims=True) + jnp.exp(limit - top)
+            weights = (raised * (1.0 / totals)).astype(bf16)
+            result = jnp.dot(weights, values, preferred_element_type=f32)
+            one, two = result[:WINDOW], result[WINDOW:]
+            if head % 2 == 0:
+                joined = jnp.where(low_half, one, pltpu.roll(two, HEAD, 1))
+            else:
+                joined = jnp.where(low_half, pltpu.roll(one, HEAD, 1), two)
+            mixer[part, hp + head * 2 * HEAD : hp + (head + 1) * 2 * HEAD] = joined.astype(bf16)
+        return carry
+
+    lax.fori_loop(0, blocks, attend, 0)
+
+    @pl.when(jnp.logical_not(inner))
+    def _():
+        pool_stage()
+
+    halo_in(2, pool_band, pool_pad)
+    level = (tp * 2 + x) * hp // (POOL // 4)
+    reach = jnp.where(level == 0, 1, jnp.where(level == 1, 2, jnp.where(level == 2, 4, 8)))
+
+    def pool(i, carry):
+        wide = WINDOW + 2 * pool_pad
+        part = pl.ds(pl.multiple_of(i * WINDOW, WINDOW), WINDOW)
+        running = pool_band[pl.ds(pl.multiple_of(i * WINDOW, pool_pad), wide), :].astype(f32)
+        chosen = None
+        for step in range(4):
+            size = 2**step
+            running = running + pltpu.roll(running, wide - size, 0)
+            shifted = pltpu.roll(running, size, 0)[pool_pad : pool_pad + WINDOW]
+            chosen = shifted if chosen is None else jnp.where(level == step, shifted, chosen)
+        spot = z * plane + i * WINDOW + lax.broadcasted_iota(jnp.int32, (WINDOW, 1), 0)
+        low = jnp.maximum(spot - reach, 0)
+        high = jnp.minimum(spot + reach - 1, seq - 1)
+        mixer[part, 0:hp] = (chosen / (high - low + 1).astype(f32)).astype(bf16)
+        return carry
+
+    lax.fori_loop(0, blocks, pool, 0)
+
+    def source_of(b):
+        group = b // 2
+        paired = jnp.minimum(z, deep - 1 - z)
+        step = jnp.where(group > 2 * paired, group - paired, (group + 1) // 2)
+        downwards = jnp.where(group > 2 * paired, 2 * z > deep - 1, group % 2 == 1)
+        return jnp.where(downwards, z - step, z + step) * 2 + b % 2
+
+    slots = kept.shape[0]
+
+    def product(source, c, which):
+        left = jnp.concatenate(
+            [
+                mixer[pl.ds(pl.multiple_of((unit * 2 + which) * share, 16), share), :]
+                for unit in range(4)
+            ],
+            axis=0,
+        )
+        return jnp.dot(left, w_out[source, c], preferred_element_type=f32).astype(bf16)
+
+    def met_copy(b, c):
+        return remote(
+            away.at[b % slots, c], met.at[b, c], met_send.at[b, c], met_recv.at[b, c], (me, tp_c)
+        )
+
+    def axes(c):
+        return (x, y) if c % 2 == 0 else (y, x)
+
+    def unit_rows(c, first, second):
+        unit = first * 2 + second if c % 2 == 0 else second * 2 + first
+        return pl.ds(pl.multiple_of(unit * share, 16), share)
+
+    def hop_copy(b, c, hop):
+        over = (c + hop) % 2 == 0
+        device = (me_x, tp) if over else (me, tp_y)
+        send, recv = (one_send, one_recv) if hop == 0 else (two_send, two_recv)
+        return remote(
+            send.at[b, c], recv.at[b, c], hop_send.at[hop, b, c], hop_recv.at[hop, b, c], device
+        )
+
+    def chip_sum(b, c, first, second):
+        part = unit_rows(c, first, second)
+        return kept[b % slots, c, part, :].astype(f32) + met[b, c, part, :].astype(f32)
+
+    def columns_of(b, c):
+        first = source_of(b) * width + c * narrow
+        return pl.ds(pl.multiple_of(first, narrow), narrow)
+
+    def done_copy(b, c):
+        return pltpu.make_async_copy(done.at[b, c], out.at[:, columns_of(b, c)], done_sem.at[b, c])
+
+    def multiply(b):
+        source = source_of(b)
+
+        @pl.when(b >= slots)
+        def _():
+            for c in range(out_parts):
+                met_copy(b - slots, c).wait_send()
+
+        for c in range(out_parts):
+            away[b % slots, c] = product(source, c, 1 - core)
+            met_copy(b, c).start()
+        for c in range(out_parts):
+            kept[b % slots, c] = product(source, c, core)
+
+    def first_hop(b):
+        for c in range(out_parts):
+            met_copy(b, c).wait_recv()
+            first, _ = axes(c)
+            for second in range(2):
+                one_send[b, c, second] = chip_sum(b, c, 1 - first, second).astype(bf16)
+            hop_copy(b, c, 0).start()
+
+    def second_hop(b):
+        for c in range(out_parts):
+            hop_copy(b, c, 0).wait_recv()
+            first, second = axes(c)
+            value = chip_sum(b, c, first, 1 - second) + one_recv[b, c, 1 - second].astype(f32)
+            two_send[b, c] = value.astype(bf16)
+            hop_copy(b, c, 1).start()
+
+    def finish(b):
+        for c in range(out_parts):
+            first, second = axes(c)
+            value = chip_sum(b, c, first, second) + one_recv[b, c, second].astype(f32)
+            hop_copy(b, c, 1).wait_recv()
+            done[b, c] = (value + two_recv[b, c].astype(f32)).astype(bf16)
+            done_copy(b, c).start()
+
+    ahead = jnp.where(inner, 0, 2 * out_parts)
+
+    def out_block(b, carry):
+        @pl.when(b < count)
+        def _():
+            low = jnp.maximum(b * out_parts - ahead, 0)
+            high = jnp.minimum((b + 1) * out_parts - ahead, all_events(out_ring))
+            events(out_ring, low, high)
+            multiply(b)
+            first_hop(b)
+
+        @pl.when((b >= 1) & (b < count + 1))
+        def _():
+            second_hop(b - 1)
+
+        @pl.when(b >= 2)
+        def _():
+            finish(b - 2)
+
+        return carry
+
+    lax.fori_loop(0, count + 2, out_block, 0)
+
+    for ring in (in_ring, pool_ring, out_ring):
+        sends_done(ring)
+    for hop in range(1, members):
+        sum_copy(tp, hop).wait_send()
+
+    def tokens_sent(j, carry):
+        over_y(0, x, tp, j).wait_send()
+        over_x(0, x, tp, j).wait_send()
+        over_core(0, x, tp, j).wait_send()
+        over_core(1, 1 - x, tp, j).wait_send()
+        over_core(2, x, tp_y, j).wait_send()
+        over_core(3, 1 - x, tp_y, j).wait_send()
+
+        @pl.when(by_x(j))
+        def _():
+            over_x(1, x, tp_y, j).wait_send()
+
+        @pl.when(jnp.logical_not(by_x(j)))
+        def _():
+            over_y(1, 1 - x, tp, j).wait_send()
+
+        return carry
+
+    lax.fori_loop(0, tiles, tokens_sent, 0)
+    for index, buffer, size in ((0, band, WINDOW), (2, pool_band, pool_pad)):
+
+        @pl.when(has_down)
+        def _(index=index, buffer=buffer, size=size):
+            halo(index, buffer, size, False).wait_send()
+
+        @pl.when(has_up)
+        def _(index=index, buffer=buffer, size=size):
+            halo(index + 1, buffer, size, True).wait_send()
+
+    def blocks_sent(b, carry):
+        for c in range(out_parts):
+
+            @pl.when(b >= count - slots)
+            def _(c=c):
+                met_copy(b, c).wait_send()
+
+            hop_copy(b, c, 0).wait_send()
+            hop_copy(b, c, 1).wait_send()
+            done_copy(b, c).wait()
+        return carry
+
+    lax.fori_loop(0, count, blocks_sent, 0)
+
+
+def plane_scratch(count, members, rows, features, depth, kw, qw, pw, width):
+    hk, hq, hp = kw // 2, qw // 2, pw // 2
+    share, narrow, plane, slots = rows // members, width // out_parts, 2 * rows, 4
+    tiles = rows // WINDOW
+    dma = pltpu.SemaphoreType.DMA
+    return [
+        pltpu.VMEM((rows, features), bf16),
+        pltpu.VMEM((members, -(-tiles // 8) * 8, WINDOW), f32),
+        pltpu.VMEM((2, count, rows, depth), bf16),
+        pltpu.VMEM((count, depth, 2 * hk + hq), bf16),
+        pltpu.VMEM((count, depth, hp), bf16),
+        pltpu.VMEM((count, out_parts, hp + hq, narrow), bf16),
+        pltpu.VMEM((depth, 2 * hk + hq), bf16),
+        pltpu.VMEM((depth, hp), bf16),
+        pltpu.VMEM((out_parts, hp + hq, narrow), bf16),
+        pltpu.VMEM((plane, 2 * hk + hq), f32),
+        pltpu.VMEM((plane, hp), f32),
+        pltpu.VMEM((plane + 2 * WINDOW, 2 * hk), bf16),
+        pltpu.VMEM((plane + 2 * pool_pad, hp), bf16),
+        pltpu.VMEM((plane, 2 * HEAD), f32),
+        pltpu.VMEM((plane, 2 * HEAD), f32),
+        pltpu.VMEM((plane, hp + hq), bf16),
+        pltpu.VMEM((slots, out_parts, 4 * share, narrow), bf16),
+        pltpu.VMEM((count, out_parts, 4 * share, narrow), bf16),
+        pltpu.VMEM((slots, out_parts, 4 * share, narrow), bf16),
+        pltpu.VMEM((count, out_parts, 2, share, narrow), bf16),
+        pltpu.VMEM((count, out_parts, 2, share, narrow), bf16),
+        pltpu.VMEM((count, out_parts, share, narrow), bf16),
+        pltpu.VMEM((count, out_parts, share, narrow), bf16),
+        pltpu.VMEM((count, out_parts, share, narrow), bf16),
+        dma((9 + 4 * out_parts,)),
+        dma((members - 1,)),
+        dma((members - 1,)),
+        dma((3, count, in_parts)),
+        dma((3, count, 1)),
+        dma((3, count, out_parts)),
+        dma((in_parts + 1 + out_parts,)),
+        dma((2, tiles)),
+        dma((2, tiles)),
+        dma((2, tiles)),
+        dma((2, tiles)),
+        dma((4, tiles)),
+        dma((4, tiles)),
+        dma((4,)),
+        dma((4,)),
+        dma((count, out_parts)),
+        dma((count, out_parts)),
+        dma((2, count, out_parts)),
+        dma((2, count, out_parts)),
+        dma((count, out_parts)),
+    ]
+
+
+def ring_scratch(count, members, rows, features, depth, kw, qw, pw, width):
+    chips, share = members // 2, rows // members
+    far = max(chips - 1, 1)
+    dma = pltpu.SemaphoreType.DMA
+    return [
+        pltpu.VMEM((members, rows, features), bf16),
+        pltpu.VMEM((count, rows, depth), bf16),
+        pltpu.VMEM((count, depth, 2 * kw + pw), bf16),
+        pltpu.VMEM((count, depth, qw), bf16),
+        pltpu.VMEM((count, pw + qw, width), bf16),
+        pltpu.VMEM((rows, 2 * kw + pw), f32),
+        pltpu.VMEM((rows, qw), f32),
+        pltpu.VMEM((rows + 2 * WINDOW, 2 * kw), bf16),
+        pltpu.VMEM((rows + 2 * pool_pad, pw), bf16),
+        pltpu.VMEM((rows, 2 * HEAD), f32),
+        pltpu.VMEM((rows, 2 * HEAD), f32),
+        pltpu.VMEM((rows, pw + qw), bf16),
+        pltpu.VMEM((count, chips * share, width), bf16),
+        pltpu.VMEM((count, chips * share, width), bf16),
+        pltpu.VMEM((count, chips * share, width), bf16),
+        pltpu.VMEM((count, far, share, width), bf16),
+        pltpu.VMEM((count, far, share, width), bf16),
+        pltpu.VMEM((count, share, width), bf16),
+        dma((7,)),
+        dma((2, count, chunks)),
+        dma((count, chunks)),
+        dma((2, count, chunks)),
+        dma((count, chunks)),
+        dma((2, count, chunks)),
+        dma((count, chunks)),
+        dma((far, token_chunks)),
+        dma((far, token_chunks)),
+        dma((chips, token_chunks)),
+        dma((chips, token_chunks)),
+        dma((4,)),
+        dma((4,)),
+        dma((count,)),
+        dma((count,)),
+        dma((count, far)),
+        dma((count, far)),
+        dma((count,)),
+    ]
+
+
 def shards(
     tokens,
     norm_gain,
@@ -657,58 +1486,28 @@
     rows, features = tokens.shape
     depth, kw = w_key.shape
     qw, pw, width = w_query.shape[1], w_pool.shape[1], w_out_pool.shape[1]
-    chips, share = members // 2, rows // members
     tables = [jnp.asarray(table) for table in rope_parts(count * rows)]
     twice = lambda gain: jnp.concatenate([gain, gain]).reshape(1, 2 * HEAD)
     anywhere = pl.BlockSpec(memory_space=pl.ANY)
     in_vmem = pl.BlockSpec(memory_space=pltpu.VMEM)
-    dma = pltpu.SemaphoreType.DMA
-    far = max(chips - 1, 1)
+    sizes = (count, members, rows, features, depth, kw, qw, pw, width)
+    shared = (
+        members == 4
+        and count % 2 == 0
+        and count >= 4
+        and rows % (2 * WINDOW) == 0
+        and depth % (16 * in_parts) == 0
+        and all(size % 256 == 0 for size in (kw, qw, pw, width))
+    )
+    kernel, scratch = (plane_kernel, plane_scratch) if shared else (layer_kernel, ring_scratch)
     return pl.pallas_call(
-        functools.partial(layer_kernel, count, members),
-        out_shape=jax.ShapeDtypeStruct((share, count * width), bf16),
+        functools.partial(kernel, count, members),
+        out_shape=jax.ShapeDtypeStruct((rows // members, count * width), bf16),
         in_specs=[anywhere] * 7 + [in_vmem] * 7 + [pl.BlockSpec(memory_space=pltpu.SMEM)],
         out_specs=anywhere,
-        scratch_shapes=[
-            pltpu.VMEM((members, rows, features), bf16),
-            pltpu.VMEM((count, rows, depth), bf16),
-            pltpu.VMEM((count, depth, 2 * kw + pw), bf16),
-            pltpu.VMEM((count, depth, qw), bf16),
-            pltpu.VMEM((count, pw + qw, width), bf16),
-            pltpu.VMEM((rows, 2 * kw + pw), f32),
-            pltpu.VMEM((rows, qw), f32),
-            pltpu.VMEM((rows + 2 * WINDOW, 2 * kw), bf16),
-            pltpu.VMEM((rows + 2 * pool_pad, pw), bf16),
-            pltpu.VMEM((rows, 2 * HEAD), f32),
-            pltpu.VMEM((rows, 2 * HEAD), f32),
-            pltpu.VMEM((rows, pw + qw), bf16),
-            pltpu.VMEM((count, chips * share, width), bf16),
-            pltpu.VMEM((count, chips * share, width), bf16),
-            pltpu.VMEM((count, chips * share, width), bf16),
-            pltpu.VMEM((count, far, share, width), bf16),
-            pltpu.VMEM((count, far, share, width), bf16),
-            pltpu.VMEM((count, share, width), bf16),
-            dma((7,)),
-            dma((2, count, chunks)),
-            dma((count, chunks)),
-            dma((2, count, chunks)),
-            dma((count, chunks)),
-            dma((2, count, chunks)),
-            dma((count, chunks)),
-            dma((far, token_chunks)),
-            dma((far, token_chunks)),
-            dma((chips, token_chunks)),
-            dma((chips, token_chunks)),
-            dma((4,)),
-            dma((4,)),
-            dma((count,)),
-            dma((count,)),
-            dma((count, far)),
-            dma((count, far)),
-            dma((count,)),
-        ],
+        scratch_shapes=scratch(*sizes),
         compiler_params=pltpu.CompilerParams(
-            collective_id=0, has_side_effects=True, vmem_limit_bytes=60 * 1024 * 1024
+            collective_id=0, has_side_effects=True, vmem_limit_bytes=62 * 1024 * 1024
         ),
     )(
         tokens,
@@ -718,7 +1517,7 @@
         w_pool,
         w_out_pool,
         w_out_attn,
-        norm_gain.reshape(1, -1),
+        norm_gain.reshape(members, -1) if shared else norm_gain.reshape(1, -1),
         twice(query_gain),
         twice(key_gain),
         *tables,

time: 189 us -> 197 us (1.042)
  the two profiles are of different devices: /device:TPU:1 before, /device:TPU:9 now
where the time goes in v1:
time: 197 us
  Pallas kernels  191 us (97%)
  local copies, waits for them, and re-layouts  4.03 us (2%)
    pallas_call x1, Pallas kernels, shards(): pl.pallas_call(functools.partial(kernel, count, members), out_shape=jax.S...  191 us

profile of v1, /device:TPU:9, one launch (start us, length us, event | category | flops | bytes accessed | tf_op | source)
XLA Modules:
  0.0 196.7 jit_solution(10921401008860946325)
XLA Ops:
  0.0 1.4 maximum_bitcast_fusion
  1.4 1.3 reshape.9.norm_gain
  2.7 191.3 %shard_map.145 = bf16[192,4096]{1,0:T(8,128)(2,1)} custom-call(bf16[768,1024]{1,0:T(8,128)(2,1)} %tokens.1, bf16[512,512]{1,0:T(8,128)(2,1)} %wq.1, bf16[512,256]{1,0:T(8,128)(2,1)} %wk.1, bf16[512,256]{1,0:T(8,128)(2,1)} %wv.1, bf16[512,256]{1,0:T(8,128)(2,1)} %wp.1, bf16[256,512]{1,0:T(8,128)(2,1)} %wop.1, bf16[512,512]{1,0:T(8,128)(2,1)} %woa.1, ...), custom_call_target="tpu_custom_call" | custom-call | tf_op jit(solution)/shard_map/pallas_call | solution.py:1503
  194.0 2.7 %copy.17 = bf16[192,4096]{1,0:T(8,128)(2,1)} copy(bf16[192,4096]{1,0:T(8,128)(2,1)} %shard_map.145) | data formatting | bytes 3145728

commit v2 on v1

--- a/solution.py
+++ b/solution.py
@@ -20,7 +20,7 @@
 chunks = 4
 token_chunks = 8
 in_parts = 4
-out_parts = 2
+pooled_parts = 4
 MESH = pl.DeviceIdType.MESH
 f32, bf16 = jnp.float32, jnp.bfloat16
 
@@ -677,14 +677,8 @@
     cosines,
     sines,
     mixer,
-    away,
-    met,
-    kept,
-    one_send,
-    one_recv,
-    two_send,
-    two_recv,
-    done,
+    result,
+    rounded,
     load_sem,
     sum_send,
     sum_recv,
@@ -692,25 +686,20 @@
     pool_sems,
     out_sems,
     x_sems,
-    tx_send,
-    tx_recv,
-    ty_send,
-    ty_recv,
-    td_send,
-    td_recv,
+    spread_sems,
+    token_sems,
+    attend_sems,
+    pooled_sems,
     halo_send,
     halo_recv,
-    met_send,
-    met_recv,
-    hop_send,
-    hop_recv,
-    done_sem,
+    result_send,
+    result_recv,
 ):
     rows, features = tokens.shape
     depth = wk.shape[0]
     hk, hq, hp = wk.shape[1] // 2, wq.shape[1] // 2, wp.shape[1] // 2
     width = wop.shape[1]
-    narrow = width // out_parts
+    narrow = width // members
     share = rows // members
     plane = 2 * rows
     heads_k = hk // HEAD
@@ -743,14 +732,17 @@
     load(tokens, raw)
     for target, pick in ((w_pool.at[me], mine), (pool_spare, other)):
         load(wp.at[:, pick(hp)], target)
-    for target, pick in ((w_out.at[me], mine), (out_spare, other)):
-        for part in range(out_parts):
-            columns = pl.ds(part * narrow, narrow)
-            load(wop.at[pick(hp), columns], target.at[part, pl.ds(0, hp), :])
-            load(woa.at[pick(hq), columns], target.at[part, pl.ds(hp, hq), :])
+    strip = lambda t: pl.ds(pl.multiple_of(t * narrow, narrow), narrow)
+    for target, t in [(w_out.at[z, tp], tp)] + [(out_spare.at[t], t) for t in range(members)]:
+        for h in range(2):
+            first = h * (hp + hq)
+            load(wop.at[pl.ds(h * hp, hp), strip(t)], target.at[pl.ds(first, hp), :])
+            load(woa.at[pl.ds(h * hq, hq), strip(t)], target.at[pl.ds(first + hp, hq), :])
 
     barrier = pltpu.get_barrier_semaphore()
-    greeted = [(up, tp), (down, tp), (me_x, tp), (me, tp_y), (me, tp_c), (me, tp_yc)]
+    greeted = [(up, tp), (down, tp), (me_x, tp)]
+    for t in (tp_y, tp_c, tp_yc):
+        greeted += [(me, t), (me_x, t)]
     for device in greeted:
         pl.semaphore_signal(barrier, inc=1, device_id=device, device_id_type=MESH)
     pl.semaphore_wait(barrier, len(greeted))
@@ -772,27 +764,17 @@
 
         return view
 
-    in_ring = (w_in, in_spare, in_sems, 0, in_parts, by_rows(in_parts), True)
-    pool_ring = (w_pool, pool_spare, pool_sems, in_parts, 1, by_rows(1), False)
-    out_ring = (
-        w_out,
-        out_spare,
-        out_sems,
-        in_parts + 1,
-        out_parts,
-        lambda buffer, c: buffer.at[c],
-        False,
-    )
-
+    in_ring = (w_in, in_spare, in_sems, 0, in_parts, by_rows(in_parts))
+    pool_ring = (w_pool, pool_spare, pool_sems, in_parts, 1, by_rows(1))
     def z_copy(ring, way, source, c):
-        buffer, _, sems, _, _, view, _ = ring
+        buffer, _, sems, _, _, view = ring
         part = view(buffer.at[source], c)
         return remote(
             part, part, sems.at[way, source, c], sems.at[2, source, c], ((up, down)[way], tp)
         )
 
     def x_copy(ring, source, c):
-        buffer, spare, sems, first, _, view, _ = ring
+        buffer, spare, sems, first, _, view = ring
         return remote(
             view(spare, c),
             view(buffer.at[source], c),
@@ -829,7 +811,7 @@
     def passing(ring, n):
         parts = ring[4]
         step, j, c = n // (2 * parts) + 1, n // parts % 2, n % parts
-        column = (x + j) % 2 if ring[6] else j
+        column = (x + j) % 2
         low, high = z - step, z + step
         return (low >= 0, low * 2 + column), (high < deep, high * 2 + column), c
 
@@ -882,6 +864,81 @@
             return carry
 
         lax.fori_loop(0, all_events(ring), body, 0)
+
+    def out_copy(way, level, c):
+        part = w_out.at[level, (tp - c + members) % members]
+        device = ((up, down)[way], tp)
+        return remote(part, part, out_sems.at[way, level, c], out_sems.at[2, level, c], device)
+
+    def spread(c):
+        target = (tp + c) % members
+        return remote(
+            out_spare.at[target],
+            w_out.at[z, tp],
+            spread_sems.at[c],
+            out_sems.at[2, z, c],
+            (me, target),
+        )
+
+    def spread_in(c):
+        owner = (tp - c + members) % members
+        return remote(
+            out_spare.at[owner],
+            w_out.at[z, owner],
+            spread_sems.at[c],
+            out_sems.at[2, z, c],
+            (me, owner),
+        )
+
+    def out_both(c, act):
+        @pl.when(has_up)
+        def _():
+            act(out_copy(0, z, c))
+
+        @pl.when(has_down)
+        def _():
+            act(out_copy(1, z, c))
+
+    def out_event(n):
+        step, c = n // members + 1, n % members
+        low, high = z - step, z + step
+
+        @pl.when(low >= 0)
+        def _():
+            out_copy(0, low, c).wait_recv()
+
+            @pl.when(has_up)
+            def _():
+                out_copy(0, low, c).start()
+
+        @pl.when(high < deep)
+        def _():
+            out_copy(1, high, c).wait_recv()
+
+            @pl.when(has_down)
+            def _():
+                out_copy(1, high, c).start()
+
+    def out_events(first, last):
+        def body(n, carry):
+            out_event(n)
+            return carry
+
+        lax.fori_loop(first, last, body, 0)
+
+    def out_sent(n, carry):
+        step, c = n // members + 1, n % members
+        low, high = z - step, z + step
+
+        @pl.when((low >= 0) & has_up)
+        def _():
+            out_copy(0, low, c).wait_send()
+
+        @pl.when((high < deep) & has_down)
+        def _():
+            out_copy(1, high, c).wait_send()
+
+        return carry
 
     for copy in loads[:6]:
         copy.wait()
@@ -921,25 +978,101 @@
         squares = squares + sums[t]
     scales = lax.rsqrt(squares / (members * features) + eps)
 
-    def token_part(side, owner, j):
-        return normed.at[
-            side,
-            pl.ds(owner * pieces, pieces),
-            pl.ds(pl.multiple_of(j * WINDOW, WINDOW), WINDOW),
-            :,
-        ]
-
-    def over_x(slot, side, owner, j):
-        part = token_part(side, owner, j)
-        return remote(part, part, tx_send.at[slot, j], tx_recv.at[slot, j], (me_x, tp))
-
-    def over_y(slot, side, owner, j):
-        part = token_part(side, owner, j)
-        return remote(part, part, ty_send.at[slot, j], ty_recv.at[slot, j], (me, tp_y))
-
-    def over_core(slot, side, owner, j):
-        part = token_part(side, owner, j)
-        return remote(part, part, td_send.at[slot, j], td_recv.at[slot, j], (me, tp_c))
+    class Stream:
+        def __init__(self, view, sems, by_x):
+            self.view, self.sems, self.by_x = view, sems, by_x
+
+        def copy(self, base, count_of, slot, side, owner, j, device):
+            part = self.view(side, owner, j)
+            send, recv = self.sems.at[base + slot, j], self.sems.at[base + count_of + slot, j]
+            return remote(part, part, send, recv, device)
+
+        def over_x(self, slot, side, owner, j):
+            return self.copy(0, 2, slot, side, owner, j, (me_x, tp))
+
+        def over_y(self, slot, side, owner, j):
+            return self.copy(4, 2, slot, side, owner, j, (me, tp_y))
+
+        def over_core(self, slot, side, owner, j):
+            return self.copy(8, 4, slot, side, owner, j, (me, tp_c))
+
+        def start(self, j):
+            self.over_y(0, x, tp, j).start()
+            self.over_x(0, x, tp, j).start()
+            self.over_core(0, x, tp, j).start()
+
+        def direct(self, j):
+            self.over_y(0, x, tp_y, j).wait_recv()
+            self.over_core(2, x, tp_y, j).start()
+
+            @pl.when(self.by_x(j))
+            def _():
+                self.over_x(1, x, tp_y, j).start()
+
+            self.over_x(0, 1 - x, tp, j).wait_recv()
+            self.over_core(1, 1 - x, tp, j).start()
+
+            @pl.when(jnp.logical_not(self.by_x(j)))
+            def _():
+                self.over_y(1, 1 - x, tp, j).start()
+
+        def crossed(self, j):
+            @pl.when(self.by_x(j))
+            def _():
+                self.over_x(1, 1 - x, tp_y, j).wait_recv()
+
+            @pl.when(jnp.logical_not(self.by_x(j)))
+            def _():
+                self.over_y(1, 1 - x, tp_y, j).wait_recv()
+
+            self.over_core(3, 1 - x, tp_y, j).start()
+
+        def near_side(self, j):
+            self.over_core(0, x, tp_c, j).wait_recv()
+            self.over_core(2, x, tp_yc, j).wait_recv()
+
+        def far_side(self, j):
+            self.over_core(1, 1 - x, tp_c, j).wait_recv()
+            self.over_core(3, 1 - x, tp_yc, j).wait_recv()
+
+        def sent(self, j):
+            self.over_y(0, x, tp, j).wait_send()
+            self.over_x(0, x, tp, j).wait_send()
+            self.over_core(0, x, tp, j).wait_send()
+            self.over_core(1, 1 - x, tp, j).wait_send()
+            self.over_core(2, x, tp_y, j).wait_send()
+            self.over_core(3, 1 - x, tp_y, j).wait_send()
+
+            @pl.when(self.by_x(j))
+            def _():
+                self.over_x(1, x, tp_y, j).wait_send()
+
+            @pl.when(jnp.logical_not(self.by_x(j)))
+            def _():
+                self.over_y(1, 1 - x, tp, j).wait_send()
+
+        def every(self, act):
+            def body(j, carry):
+                act(j)
+                return carry
+
+            lax.fori_loop(0, self.sems.shape[1], body, 0)
+
+    def block_rows(j, size):
+        return pl.ds(pl.multiple_of(j * size, 16), size)
+
+    def token_view(side, owner, j):
+        return normed.at[side, pl.ds(owner * pieces, pieces), block_rows(j, WINDOW), :]
+
+    def attend_view(side, owner, j):
+        return mixer.at[owner, side, block_rows(j, WINDOW), pl.ds(hp, hq)]
+
+    def pooled_view(side, owner, j):
+        return mixer.at[owner, side, block_rows(j, plane // pooled_parts), pl.ds(0, hp)]
+
+    token_stream = Stream(token_view, token_sems, lambda j: j % 3 == 0)
+    attend_stream = Stream(attend_view, attend_sems, lambda j: j % 2 == 0)
+    pooled_stream = Stream(pooled_view, pooled_sems, lambda j: j % 2 == 0)
 
     gains = norm_gain[pl.ds(tp, 1), :]
     for i in range(tiles):
@@ -950,33 +1083,15 @@
             value = (block * scale * gains[:, first : first + WINDOW]).astype(bf16)
             inside = first % depth
             normed[x, tp * pieces + first // depth, here, inside : inside + WINDOW] = value
-        over_y(0, x, tp, i).start()
-        over_x(0, x, tp, i).start()
-        over_core(0, x, tp, i).start()
+        token_stream.start(i)
 
     side_in(in_ring)
     whole = all_events(in_ring)
     reached = lambda part: whole * part // 24
     events(in_ring, 0, reached(4))
 
-    def by_x(j):
-        return j % 3 == 0
-
     def direct(j, carry):
-        over_y(0, x, tp_y, j).wait_recv()
-        over_core(2, x, tp_y, j).start()
-
-        @pl.when(by_x(j))
-        def _():
-            over_x(1, x, tp_y, j).start()
-
-        over_x(0, 1 - x, tp, j).wait_recv()
-        over_core(1, 1 - x, tp, j).start()
-
-        @pl.when(jnp.logical_not(by_x(j)))
-        def _():
-            over_y(1, 1 - x, tp, j).start()
-
+        token_stream.direct(j)
         events(in_ring, reached(4 + 12 * j // tiles), reached(4 + 12 * (j + 1) // tiles))
         return carry
 
@@ -984,44 +1099,21 @@
     for copy in loads[7:]:
         copy.wait()
     side_out(pool_ring)
-    side_out(out_ring)
-
-    def crossed(j, carry):
-        @pl.when(by_x(j))
-        def _():
-            over_x(1, 1 - x, tp_y, j).wait_recv()
-
-        @pl.when(jnp.logical_not(by_x(j)))
-        def _():
-            over_y(1, 1 - x, tp_y, j).wait_recv()
-
-        over_core(3, 1 - x, tp_y, j).start()
-        events(in_ring, reached(16 + 6 * j // tiles), reached(16 + 6 * (j + 1) // tiles))
-        return carry
-
-    lax.fori_loop(0, tiles, crossed, 0)
-    own_out(pool_ring)
-
-    def from_core(j, carry):
-        over_core(0, x, tp_c, j).wait_recv()
-        over_core(1, 1 - x, tp_c, j).wait_recv()
-        over_core(2, x, tp_yc, j).wait_recv()
-        over_core(3, 1 - x, tp_yc, j).wait_recv()
-        return carry
-
-    lax.fori_loop(0, tiles, from_core, 0)
+    for c in range(1, members):
+        spread(c).start()
+    token_stream.every(token_stream.near_side)
 
     tile_rows = 256 if rows % 256 == 0 else 128
     per_side = rows // tile_rows
 
-    def project(result, weights, level, first=False):
+    def project(result, weights, level, side, first=False):
         def body(i, carry):
-            part = pl.ds(pl.multiple_of(i * tile_rows, tile_rows), tile_rows)
-            within = pl.ds(pl.multiple_of(i % per_side * tile_rows, tile_rows), tile_rows)
+            within = pl.ds(pl.multiple_of(i * tile_rows, tile_rows), tile_rows)
+            part = pl.ds(pl.multiple_of(side * rows + i * tile_rows, tile_rows), tile_rows)
             value = None if first else result[part, :]
             for j in range(2):
                 term = jnp.dot(
-                    normed[i // per_side, level * 2 + j, within, :],
+                    normed[side, level * 2 + j, within, :],
                     weights[level * 2 + j],
                     preferred_element_type=f32,
                 )
@@ -1029,23 +1121,48 @@
             result[part, :] = value
             return carry
 
-        lax.fori_loop(0, 2 * per_side, body, 0)
-
-    def project_step(result, weights, step):
+        lax.fori_loop(0, per_side, body, 0)
+
+    def project_step(result, weights, step, side):
         @pl.when(z - step >= 0)
         def _():
-            project(result, weights, z - step)
+            project(result, weights, z - step, side)
 
         @pl.when(z + step < deep)
         def _():
-            project(result, weights, z + step)
-
-    project(total, w_in, z, first=True)
+            project(result, weights, z + step, side)
+
+    early = max(reached(16) // (2 * in_parts), 0)
+
+    def crossed(j, carry):
+        token_stream.crossed(j)
+
+        @pl.when(j == 0)
+        def _():
+            project(total, w_in, z, x, first=True)
+
+        @pl.when((j >= 1) & (j <= early))
+        def _():
+            project_step(total, w_in, j, x)
+
+        events(in_ring, reached(16 + 6 * j // tiles), reached(16 + 6 * (j + 1) // tiles))
+        return carry
+
+    lax.fori_loop(0, tiles, crossed, 0)
+    own_out(pool_ring)
+    side_in(pool_ring)
+    token_stream.every(token_stream.far_side)
+    project(total, w_in, z, 1 - x, first=True)
 
     def in_step(step, carry):
         each = 2 * in_parts
         events(in_ring, jnp.maximum((step - 1) * each, reached(22)), step * each)
-        project_step(total, w_in, step)
+
+        @pl.when(step > min(early, tiles - 1))
+        def _():
+            project_step(total, w_in, step, x)
+
+        project_step(total, w_in, step, 1 - x)
         return carry
 
     lax.fori_loop(1, deep, in_step, 0)
@@ -1113,12 +1230,13 @@
     halo_out(0, band, WINDOW)
 
     def pool_stage():
-        side_in(pool_ring)
-        project(pool_total, w_pool, z, first=True)
+        for side in range(2):
+            project(pool_total, w_pool, z, side, first=True)
 
         def step_body(step, carry):
             events(pool_ring, (step - 1) * 2, step * 2)
-            project_step(pool_total, w_pool, step)
+            for side in range(2):
+                project_step(pool_total, w_pool, step, side)
             return carry
 
         lax.fori_loop(1, deep, step_body, 0)
@@ -1129,8 +1247,10 @@
     def _():
         pool_stage()
 
-    own_out(out_ring)
-    side_in(out_ring)
+    out_both(0, start)
+    for c in range(1, members):
+        spread_in(c).wait_recv()
+        out_both(c, start)
 
     row = lax.broadcasted_iota(jnp.int32, (2 * WINDOW, 3 * WINDOW), 0) % WINDOW
     column = lax.broadcasted_iota(jnp.int32, (2 * WINDOW, 3 * WINDOW), 1)
@@ -1181,10 +1301,24 @@
                 joined = jnp.where(low_half, one, pltpu.roll(two, HEAD, 1))
             else:
                 joined = jnp.where(low_half, pltpu.roll(one, HEAD, 1), two)
-            mixer[part, hp + head * 2 * HEAD : hp + (head + 1) * 2 * HEAD] = joined.astype(bf16)
-        return carry
-
+            lanes = slice(hp + head * 2 * HEAD, hp + (head + 1) * 2 * HEAD)
+            mixer[tp, x, part, lanes] = joined.astype(bf16)
+        attend_stream.start(i)
+
+        @pl.when(turn >= behind)
+        def _():
+            attend_stream.direct((turn - behind + 1) % blocks)
+
+        return carry
+
+    behind = 2
     lax.fori_loop(0, blocks, attend, 0)
+    for turn in range(blocks - behind, blocks):
+        attend_stream.direct((turn + 1) % blocks)
+
+    @pl.when(inner)
+    def _():
+        out_events(0, members)
 
     @pl.when(jnp.logical_not(inner))
     def _():
@@ -1207,146 +1341,117 @@
         spot = z * plane + i * WINDOW + lax.broadcasted_iota(jnp.int32, (WINDOW, 1), 0)
         low = jnp.maximum(spot - reach, 0)
         high = jnp.minimum(spot + reach - 1, seq - 1)
-        mixer[part, 0:hp] = (chosen / (high - low + 1).astype(f32)).astype(bf16)
+        mixer[tp, x, part, 0:hp] = (chosen / (high - low + 1).astype(f32)).astype(bf16)
         return carry
 
     lax.fori_loop(0, blocks, pool, 0)
 
-    def source_of(b):
-        group = b // 2
+    pooled_stream.every(pooled_stream.start)
+    attend_stream.every(attend_stream.crossed)
+    pooled_stream.every(pooled_stream.direct)
+    pooled_stream.every(pooled_stream.crossed)
+    for stream in (attend_stream, pooled_stream):
+        stream.every(stream.near_side)
+        stream.every(stream.far_side)
+
+    def level_of(group):
         paired = jnp.minimum(z, deep - 1 - z)
         step = jnp.where(group > 2 * paired, group - paired, (group + 1) // 2)
         downwards = jnp.where(group > 2 * paired, 2 * z > deep - 1, group % 2 == 1)
-        return jnp.where(downwards, z - step, z + step) * 2 + b % 2
-
-    slots = kept.shape[0]
-
-    def product(source, c, which):
-        left = jnp.concatenate(
-            [
-                mixer[pl.ds(pl.multiple_of((unit * 2 + which) * share, 16), share), :]
-                for unit in range(4)
-            ],
-            axis=0,
+        return jnp.where(downwards, z - step, z + step)
+
+    here = x * members + tp
+    out_steps = (deep - 1) * members
+
+    def columns_of(level, side, t):
+        first = (level * 2 + side) * width + t * narrow
+        return pl.ds(pl.multiple_of(first, narrow), narrow)
+
+    def result_copy(level, hop):
+        target = (here + hop) % (2 * members)
+        return remote(
+            rounded.at[level, pl.ds(pl.multiple_of(target * share, 16), share), :],
+            out.at[:, columns_of(level, x, tp)],
+            result_send.at[level, hop],
+            result_recv.at[level, hop],
+            (z * 2 + target // members, target % members),
         )
-        return jnp.dot(left, w_out[source, c], preferred_element_type=f32).astype(bf16)
-
-    def met_copy(b, c):
+
+    def result_in(level, hop):
+        source = (here - hop + 2 * members) % (2 * members)
         return remote(
-            away.at[b % slots, c], met.at[b, c], met_send.at[b, c], met_recv.at[b, c], (me, tp_c)
+            rounded.at[level, pl.ds(0, share), :],
+            out.at[:, columns_of(level, source // members, source % members)],
+            result_send.at[level, hop],
+            result_recv.at[level, hop],
+            (z * 2 + source // members, source % members),
         )
 
-    def axes(c):
-        return (x, y) if c % 2 == 0 else (y, x)
-
-    def unit_rows(c, first, second):
-        unit = first * 2 + second if c % 2 == 0 else second * 2 + first
-        return pl.ds(pl.multiple_of(unit * share, 16), share)
-
-    def hop_copy(b, c, hop):
-        over = (c + hop) % 2 == 0
-        device = (me_x, tp) if over else (me, tp_y)
-        send, recv = (one_send, one_recv) if hop == 0 else (two_send, two_recv)
-        return remote(
-            send.at[b, c], recv.at[b, c], hop_send.at[hop, b, c], hop_recv.at[hop, b, c], device
+    def result_own(level):
+        return pltpu.make_async_copy(
+            rounded.at[level, pl.ds(pl.multiple_of(here * share, 16), share), :],
+            out.at[:, columns_of(level, x, tp)],
+            result_send.at[level, 0],
         )
 
-    def chip_sum(b, c, first, second):
-        part = unit_rows(c, first, second)
-        return kept[b % slots, c, part, :].astype(f32) + met[b, c, part, :].astype(f32)
-
-    def columns_of(b, c):
-        first = source_of(b) * width + c * narrow
-        return pl.ds(pl.multiple_of(first, narrow), narrow)
-
-    def done_copy(b, c):
-        return pltpu.make_async_copy(done.at[b, c], out.at[:, columns_of(b, c)], done_sem.at[b, c])
-
-    def multiply(b):
-        source = source_of(b)
-
-        @pl.when(b >= slots)
-        def _():
-            for c in range(out_parts):
-                met_copy(b - slots, c).wait_send()
-
-        for c in range(out_parts):
-            away[b % slots, c] = product(source, c, 1 - core)
-            met_copy(b, c).start()
-        for c in range(out_parts):
-            kept[b % slots, c] = product(source, c, core)
-
-    def first_hop(b):
-        for c in range(out_parts):
-            met_copy(b, c).wait_recv()
-            first, _ = axes(c)
-            for second in range(2):
-                one_send[b, c, second] = chip_sum(b, c, 1 - first, second).astype(bf16)
-            hop_copy(b, c, 0).start()
-
-    def second_hop(b):
-        for c in range(out_parts):
-            hop_copy(b, c, 0).wait_recv()
-            first, second = axes(c)
-            value = chip_sum(b, c, first, 1 - second) + one_recv[b, c, 1 - second].astype(f32)
-            two_send[b, c] = value.astype(bf16)
-            hop_copy(b, c, 1).start()
-
-    def finish(b):
-        for c in range(out_parts):
-            first, second = axes(c)
-            value = chip_sum(b, c, first, second) + one_recv[b, c, second].astype(f32)
-            hop_copy(b, c, 1).wait_recv()
-            done[b, c] = (value + two_recv[b, c].astype(f32)).astype(bf16)
-            done_copy(b, c).start()
-
-    ahead = jnp.where(inner, 0, 2 * out_parts)
-
-    def out_block(b, carry):
-        @pl.when(b < count)
-        def _():
-            low = jnp.maximum(b * out_parts - ahead, 0)
-            high = jnp.minimum((b + 1) * out_parts - ahead, all_events(out_ring))
-            events(out_ring, low, high)
-            multiply(b)
-            first_hop(b)
-
-        @pl.when((b >= 1) & (b < count + 1))
-        def _():
-            second_hop(b - 1)
-
-        @pl.when(b >= 2)
-        def _():
-            finish(b - 2)
-
-        return carry
-
-    lax.fori_loop(0, count + 2, out_block, 0)
-
-    for ring in (in_ring, pool_ring, out_ring):
+    def out_level(group, carry):
+        level = level_of(group)
+        for c in range(members):
+            first_event = jnp.where(inner, out_steps, (group - 1) * members + c)
+
+            @pl.when((first_event >= 0) & (first_event < out_steps))
+            def _():
+                out_event(first_event)
+
+            t = (tp - c + members) % members
+
+            def body(i, inner_carry):
+                part = pl.ds(pl.multiple_of(i * tile_rows, tile_rows), tile_rows)
+                value = None if c == 0 else result[part, :]
+                for h in range(2):
+                    term = jnp.dot(
+                        mixer[t, h, part, :],
+                        w_out[level, t, h * (hp + hq) : (h + 1) * (hp + hq), :],
+                        preferred_element_type=f32,
+                    )
+                    value = term if value is None else value + term
+                if c == members - 1:
+                    rounded[level, part, :] = value.astype(bf16)
+                else:
+                    result[part, :] = value
+                return inner_carry
+
+            lax.fori_loop(0, plane // tile_rows, body, 0)
+        for hop in range(1, 2 * members):
+            result_copy(level, hop).start()
+        result_own(level).start()
+        return carry
+
+    @pl.when(inner)
+    def _():
+        out_events(members, out_steps)
+
+    lax.fori_loop(0, deep, out_level, 0)
+
+    def results(level, carry):
+        for hop in range(1, 2 * members):
+            result_in(level, hop).wait_recv()
+        return carry
+
+    lax.fori_loop(0, deep, results, 0)
+
+    for ring in (in_ring, pool_ring):
         sends_done(ring)
+    for c in range(members):
+        out_both(c, sent)
+    for c in range(1, members):
+        spread(c).wait_send()
+    lax.fori_loop(0, out_steps, out_sent, 0)
     for hop in range(1, members):
         sum_copy(tp, hop).wait_send()
 
-    def tokens_sent(j, carry):
-        over_y(0, x, tp, j).wait_send()
-        over_x(0, x, tp, j).wait_send()
-        over_core(0, x, tp, j).wait_send()
-        over_core(1, 1 - x, tp, j).wait_send()
-        over_core(2, x, tp_y, j).wait_send()
-        over_core(3, 1 - x, tp_y, j).wait_send()
-
-        @pl.when(by_x(j))
-        def _():
-            over_x(1, x, tp_y, j).wait_send()
-
-        @pl.when(jnp.logical_not(by_x(j)))
-        def _():
-            over_y(1, 1 - x, tp, j).wait_send()
-
-        return carry
-
-    lax.fori_loop(0, tiles, tokens_sent, 0)
+    for stream in (token_stream, attend_stream, pooled_stream):
+        stream.every(stream.sent)
     for index, buffer, size in ((0, band, WINDOW), (2, pool_band, pool_pad)):
 
         @pl.when(has_down)
@@ -1357,25 +1462,18 @@
         def _(index=index, buffer=buffer, size=size):
             halo(index + 1, buffer, size, True).wait_send()
 
-    def blocks_sent(b, carry):
-        for c in range(out_parts):
-
-            @pl.when(b >= count - slots)
-            def _(c=c):
-                met_copy(b, c).wait_send()
-
-            hop_copy(b, c, 0).wait_send()
-            hop_copy(b, c, 1).wait_send()
-            done_copy(b, c).wait()
-        return carry
-
-    lax.fori_loop(0, count, blocks_sent, 0)
+    def results_sent(level, carry):
+        for hop in range(1, 2 * members):
+            result_copy(level, hop).wait_send()
+        result_own(level).wait()
+        return carry
+
+    lax.fori_loop(0, deep, results_sent, 0)
 
 
 def plane_scratch(count, members, rows, features, depth, kw, qw, pw, width):
     hk, hq, hp = kw // 2, qw // 2, pw // 2
-    share, narrow, plane, slots = rows // members, width // out_parts, 2 * rows, 4
-    tiles = rows // WINDOW
+    narrow, plane, deep, tiles = width // members, 2 * rows, count // 2, rows // WINDOW
     dma = pltpu.SemaphoreType.DMA
     return [
         pltpu.VMEM((rows, features), bf16),
@@ -1383,45 +1481,34 @@
         pltpu.VMEM((2, count, rows, depth), bf16),
         pltpu.VMEM((count, depth, 2 * hk + hq), bf16),
         pltpu.VMEM((count, depth, hp), bf16),
-        pltpu.VMEM((count, out_parts, hp + hq, narrow), bf16),
+        pltpu.VMEM((deep, members, 2 * (hp + hq), narrow), bf16),
         pltpu.VMEM((depth, 2 * hk + hq), bf16),
         pltpu.VMEM((depth, hp), bf16),
-        pltpu.VMEM((out_parts, hp + hq, narrow), bf16),
+        pltpu.VMEM((members, 2 * (hp + hq), narrow), bf16),
         pltpu.VMEM((plane, 2 * hk + hq), f32),
         pltpu.VMEM((plane, hp), f32),
         pltpu.VMEM((plane + 2 * WINDOW, 2 * hk), bf16),
         pltpu.VMEM((plane + 2 * pool_pad, hp), bf16),
         pltpu.VMEM((plane, 2 * HEAD), f32),
         pltpu.VMEM((plane, 2 * HEAD), f32),
-        pltpu.VMEM((plane, hp + hq), bf16),
-        pltpu.VMEM((slots, out_parts, 4 * share, narrow), bf16),
-        pltpu.VMEM((count, out_parts, 4 * share, narrow), bf16),
-        pltpu.VMEM((slots, out_parts, 4 * share, narrow), bf16),
-        pltpu.VMEM((count, out_parts, 2, share, narrow), bf16),
-        pltpu.VMEM((count, out_parts, 2, share, narrow), bf16),
-        pltpu.VMEM((count, out_parts, share, narrow), bf16),
-        pltpu.VMEM((count, out_parts, share, narrow), bf16),
-        pltpu.VMEM((count, out_parts, share, narrow), bf16),
-        dma((9 + 4 * out_parts,)),
+        pltpu.VMEM((members, 2, plane, hp + hq), bf16),
+        pltpu.VMEM((plane, narrow), f32),
+        pltpu.VMEM((deep, plane, narrow), bf16),
+        dma((13 + 4 * members,)),
         dma((members - 1,)),
         dma((members - 1,)),
         dma((3, count, in_parts)),
         dma((3, count, 1)),
-        dma((3, count, out_parts)),
-        dma((in_parts + 1 + out_parts,)),
-        dma((2, tiles)),
-        dma((2, tiles)),
-        dma((2, tiles)),
-        dma((2, tiles)),
-        dma((4, tiles)),
-        dma((4, tiles)),
+        dma((3, deep, members)),
+        dma((in_parts + 1,)),
+        dma((members,)),
+        dma((16, tiles)),
+        dma((16, 2 * tiles)),
+        dma((16, pooled_parts)),
         dma((4,)),
         dma((4,)),
-        dma((count, out_parts)),
-        dma((count, out_parts)),
-        dma((2, count, out_parts)),
-        dma((2, count, out_parts)),
-        dma((count, out_parts)),
+        dma((deep, 2 * members)),
+        dma((deep, 2 * members)),
     ]
 
 
@@ -1497,7 +1584,8 @@
         and count >= 4
         and rows % (2 * WINDOW) == 0
         and depth % (16 * in_parts) == 0
-        and all(size % 256 == 0 for size in (kw, qw, pw, width))
+        and all(size % 256 == 0 for size in (kw, qw, pw))
+        and width % (128 * members) == 0
     )
     kernel, scratch = (plane_kernel, plane_scratch) if shared else (layer_kernel, ring_scratch)
     return pl.pallas_call(

time: 197 us -> 177 us (0.90)
  the two profiles are of different devices: /device:TPU:9 before, /device:TPU:1 now
where the time goes in v2:
time: 177 us; the launch traced here: 176 us
  Pallas kernels  170 us (96%)
  local copies, waits for them, and re-layouts  4.03 us (2%)
    pallas_call x1, Pallas kernels, shards(): pl.pallas_call(functools.partial(kernel, count, members), out_shape=jax.S...  170 us

profile of v2, /device:TPU:1, one launch (start us, length us, event | category | flops | bytes accessed | tf_op | source)
XLA Modules:
  0.0 175.9 jit_solution(13732668969776707748)
XLA Ops:
  0.0 1.4 maximum_bitcast_fusion
  1.4 1.3 reshape.9.norm_gain
  2.7 170.5 %shard_map.145 = bf16[192,4096]{1,0:T(8,128)(2,1)} custom-call(bf16[768,1024]{1,0:T(8,128)(2,1)} %tokens.1, bf16[512,512]{1,0:T(8,128)(2,1)} %wq.1, bf16[512,256]{1,0:T(8,128)(2,1)} %wk.1, bf16[512,256]{1,0:T(8,128)(2,1)} %wv.1, bf16[512,256]{1,0:T(8,128)(2,1)} %wp.1, bf16[256,512]{1,0:T(8,128)(2,1)} %wop.1, bf16[512,512]{1,0:T(8,128)(2,1)} %woa.1, ...), custom_call_target="tpu_custom_call" | custom-call | tf_op jit(solution)/shard_map/pallas_call | solution.py:1591
  173.2 2.7 %copy.17 = bf16[192,4096]{1,0:T(8,128)(2,1)} copy(bf16[192,4096]{1,0:T(8,128)(2,1)} %shard_map.145) | data formatting | bytes 3145728

commit v3 on v2

--- a/solution.py
+++ b/solution.py
@@ -363,6 +363,8 @@
     opposite(side_ring)
     project(side, w_side, [at(count // 2)])
 
+    twice = lambda gain: jnp.concatenate([gain[...], gain[...]], axis=1)
+    query_gains, key_gains = twice(query_gain), twice(key_gain)
     lane = lax.broadcasted_iota(jnp.int32, (WINDOW, 2 * HEAD), 1)
     low_half = lane < HEAD
     lead = lane % (HEAD // 2) < HEAD // 4
@@ -373,7 +375,7 @@
         for h in range(kw // (2 * HEAD)):
             lanes = slice(h * 2 * HEAD, (h + 1) * 2 * HEAD)
             key = norm_rope(
-                side[part, lanes], key_gain[...], cosines[part, :], sines[part, :], low_half, lead
+                side[part, lanes], key_gains, cosines[part, :], sines[part, :], low_half, lead
             )
             band[shifted, lanes] = key.astype(bf16)
         band[shifted, kw : 2 * kw] = side[part, kw : 2 * kw].astype(bf16)
@@ -482,7 +484,7 @@
             lanes = slice(head * 2 * HEAD, (head + 1) * 2 * HEAD)
             rotated = norm_rope(
                 query[part, lanes],
-                query_gain[...],
+                query_gains,
                 cosines[part, :],
                 sines[part, :],
                 low_half,
@@ -671,12 +673,12 @@
     pool_spare,
     out_spare,
     total,
-    pool_total,
     band,
     pool_band,
     cosines,
     sines,
-    mixer,
+    attended,
+    pooled,
     result,
     rounded,
     load_sem,
@@ -734,10 +736,8 @@
         load(wp.at[:, pick(hp)], target)
     strip = lambda t: pl.ds(pl.multiple_of(t * narrow, narrow), narrow)
     for target, t in [(w_out.at[z, tp], tp)] + [(out_spare.at[t], t) for t in range(members)]:
-        for h in range(2):
-            first = h * (hp + hq)
-            load(wop.at[pl.ds(h * hp, hp), strip(t)], target.at[pl.ds(first, hp), :])
-            load(woa.at[pl.ds(h * hq, hq), strip(t)], target.at[pl.ds(first + hp, hq), :])
+        load(woa.at[:, strip(t)], target.at[pl.ds(0, 2 * hq), :])
+        load(wop.at[:, strip(t)], target.at[pl.ds(2 * hq, 2 * hp), :])
 
     barrier = pltpu.get_barrier_semaphore()
     greeted = [(up, tp), (down, tp), (me_x, tp)]
@@ -1065,10 +1065,10 @@
         return normed.at[side, pl.ds(owner * pieces, pieces), block_rows(j, WINDOW), :]
 
     def attend_view(side, owner, j):
-        return mixer.at[owner, side, block_rows(j, WINDOW), pl.ds(hp, hq)]
+        return attended.at[owner, side, block_rows(j, WINDOW), :]
 
     def pooled_view(side, owner, j):
-        return mixer.at[owner, side, block_rows(j, plane // pooled_parts), pl.ds(0, hp)]
+        return pooled.at[owner, side, block_rows(j, plane // pooled_parts), :]
 
     token_stream = Stream(token_view, token_sems, lambda j: j % 3 == 0)
     attend_stream = Stream(attend_view, attend_sems, lambda j: j % 2 == 0)
@@ -1145,7 +1145,7 @@
         def _():
             project_step(total, w_in, j, x)
 
-        events(in_ring, reached(16 + 6 * j // tiles), reached(16 + 6 * (j + 1) // tiles))
+        events(in_ring, reached(16 + 4 * j // tiles), reached(16 + 4 * (j + 1) // tiles))
         return carry
 
     lax.fori_loop(0, tiles, crossed, 0)
@@ -1154,9 +1154,14 @@
     token_stream.every(token_stream.far_side)
     project(total, w_in, z, 1 - x, first=True)
 
+    @pl.when(inner)
+    def _():
+        events(pool_ring, 0, 2)
+
+
     def in_step(step, carry):
         each = 2 * in_parts
-        events(in_ring, jnp.maximum((step - 1) * each, reached(22)), step * each)
+        events(in_ring, jnp.maximum((step - 1) * each, reached(20)), step * each)
 
         @pl.when(step > min(early, tiles - 1))
         def _():
@@ -1167,6 +1172,8 @@
 
     lax.fori_loop(1, deep, in_step, 0)
 
+    twice = lambda gain: jnp.concatenate([gain[...], gain[...]], axis=1)
+    query_gains, key_gains = twice(query_gain), twice(key_gain)
     lane = lax.broadcasted_iota(jnp.int32, (WINDOW, 2 * HEAD), 1)
     low_half = lane < HEAD
     lead = lane % (HEAD // 2) < HEAD // 4
@@ -1178,7 +1185,7 @@
         for h in range(hk // (2 * HEAD)):
             lanes = slice(h * 2 * HEAD, (h + 1) * 2 * HEAD)
             key = norm_rope(
-                total[part, lanes], key_gain[...], cosines[part, :], sines[part, :], low_half, lead
+                total[part, lanes], key_gains, cosines[part, :], sines[part, :], low_half, lead
             )
             band[shifted, lanes] = key.astype(bf16)
         band[shifted, hk:] = total[part, hk : 2 * hk].astype(bf16)
@@ -1229,27 +1236,13 @@
 
     halo_out(0, band, WINDOW)
 
-    def pool_stage():
-        for side in range(2):
-            project(pool_total, w_pool, z, side, first=True)
-
-        def step_body(step, carry):
-            events(pool_ring, (step - 1) * 2, step * 2)
-            for side in range(2):
-                project_step(pool_total, w_pool, step, side)
-            return carry
-
-        lax.fori_loop(1, deep, step_body, 0)
-        pool_band[pool_pad : pool_pad + plane, :] = pool_total[...].astype(bf16)
-        halo_out(2, pool_band, pool_pad)
-
     @pl.when(inner)
     def _():
-        pool_stage()
-
-    out_both(0, start)
-    for c in range(1, members):
-        spread_in(c).wait_recv()
+        events(pool_ring, 2, all_events(pool_ring))
+
+    for c in range(members - 1):
+        if c > 0:
+            spread_in(c).wait_recv()
         out_both(c, start)
 
     row = lax.broadcasted_iota(jnp.int32, (2 * WINDOW, 3 * WINDOW), 0) % WINDOW
@@ -1270,7 +1263,7 @@
             lanes = slice(2 * hk + head * 2 * HEAD, 2 * hk + (head + 1) * 2 * HEAD)
             rotated = norm_rope(
                 total[part, lanes],
-                query_gain[...],
+                query_gains,
                 cosines[part, :],
                 sines[part, :],
                 low_half,
@@ -1301,8 +1294,7 @@
                 joined = jnp.where(low_half, one, pltpu.roll(two, HEAD, 1))
             else:
                 joined = jnp.where(low_half, pltpu.roll(one, HEAD, 1), two)
-            lanes = slice(hp + head * 2 * HEAD, hp + (head + 1) * 2 * HEAD)
-            mixer[tp, x, part, lanes] = joined.astype(bf16)
+            attended[tp, x, part, head * 2 * HEAD : (head + 1) * 2 * HEAD] = joined.astype(bf16)
         attend_stream.start(i)
 
         @pl.when(turn >= behind)
@@ -1311,20 +1303,31 @@
 
         return carry
 
-    behind = 2
+    behind = 5
     lax.fori_loop(0, blocks, attend, 0)
-    for turn in range(blocks - behind, blocks):
-        attend_stream.direct((turn + 1) % blocks)
+
+    events(pool_ring, jnp.where(inner, all_events(pool_ring), 0), all_events(pool_ring))
+
+    for side in range(2):
+
+        def pool_project(i, carry, side=side):
+            part = pl.ds(pl.multiple_of(i * tile_rows, tile_rows), tile_rows)
+            first = side * rows + pool_pad + i * tile_rows
+            left = jnp.concatenate([normed[side, source, part, :] for source in range(count)], axis=1)
+            right = w_pool[...].reshape(count * depth, hp)
+            value = jnp.dot(left, right, preferred_element_type=f32)
+            pool_band[pl.ds(pl.multiple_of(first, pool_pad), tile_rows), :] = value.astype(bf16)
+            return carry
+
+        lax.fori_loop(0, per_side, pool_project, 0)
+    halo_out(2, pool_band, pool_pad)
+    spread_in(members - 1).wait_recv()
+    out_both(members - 1, start)
 
     @pl.when(inner)
     def _():
-        out_events(0, members)
-
-    @pl.when(jnp.logical_not(inner))
-    def _():
-        pool_stage()
-
-    halo_in(2, pool_band, pool_pad)
+        out_events(0, members - 1)
+
     level = (tp * 2 + x) * hp // (POOL // 4)
     reach = jnp.where(level == 0, 1, jnp.where(level == 1, 2, jnp.where(level == 2, 4, 8)))
 
@@ -1341,18 +1344,28 @@
         spot = z * plane + i * WINDOW + lax.broadcasted_iota(jnp.int32, (WINDOW, 1), 0)
         low = jnp.maximum(spot - reach, 0)
         high = jnp.minimum(spot + reach - 1, seq - 1)
-        mixer[tp, x, part, 0:hp] = (chosen / (high - low + 1).astype(f32)).astype(bf16)
-        return carry
-
-    lax.fori_loop(0, blocks, pool, 0)
-
-    pooled_stream.every(pooled_stream.start)
+        pooled[tp, x, part, :] = (chosen / (high - low + 1).astype(f32)).astype(bf16)
+        return carry
+
+    edge = blocks // pooled_parts
+    lax.fori_loop(edge, blocks - edge, pool, 0)
+    for part in range(1, pooled_parts - 1):
+        pooled_stream.start(part)
+    for turn in range(blocks - behind, blocks):
+        attend_stream.direct((turn + 1) % blocks)
+    halo_in(2, pool_band, pool_pad)
+    lax.fori_loop(0, edge, pool, 0)
+    lax.fori_loop(blocks - edge, blocks, pool, 0)
+    pooled_stream.start(0)
+    pooled_stream.start(pooled_parts - 1)
+
+    @pl.when(inner)
+    def _():
+        out_events(members - 1, members)
+
     attend_stream.every(attend_stream.crossed)
-    pooled_stream.every(pooled_stream.direct)
-    pooled_stream.every(pooled_stream.crossed)
-    for stream in (attend_stream, pooled_stream):
-        stream.every(stream.near_side)
-        stream.every(stream.far_side)
+    for stream_side in (attend_stream.near_side, attend_stream.far_side):
+        attend_stream.every(stream_side)
 
     def level_of(group):
         paired = jnp.minimum(z, deep - 1 - z)
@@ -1394,51 +1407,91 @@
             result_send.at[level, 0],
         )
 
-    def out_level(group, carry):
-        level = level_of(group)
-        for c in range(members):
-            first_event = jnp.where(inner, out_steps, (group - 1) * members + c)
-
-            @pl.when((first_event >= 0) & (first_event < out_steps))
-            def _():
-                out_event(first_event)
-
-            t = (tp - c + members) % members
-
-            def body(i, inner_carry):
-                part = pl.ds(pl.multiple_of(i * tile_rows, tile_rows), tile_rows)
-                value = None if c == 0 else result[part, :]
-                for h in range(2):
-                    term = jnp.dot(
-                        mixer[t, h, part, :],
-                        w_out[level, t, h * (hp + hq) : (h + 1) * (hp + hq), :],
-                        preferred_element_type=f32,
-                    )
-                    value = term if value is None else value + term
-                if c == members - 1:
-                    rounded[level, part, :] = value.astype(bf16)
-                else:
-                    result[part, :] = value
-                return inner_carry
-
-            lax.fori_loop(0, plane // tile_rows, body, 0)
+    def send_level(level):
         for hop in range(1, 2 * members):
             result_copy(level, hop).start()
         result_own(level).start()
-        return carry
+
+    span = 2 * tile_rows if plane % (2 * tile_rows) == 0 else tile_rows
+    ends_event = lambda n: jnp.where(inner, out_steps, n)
+
+    def end_events(first, last):
+        out_events(ends_event(first), ends_event(last))
+
+    def by_span(act):
+        def body(i, carry):
+            act(pl.ds(pl.multiple_of(i * span, span), span))
+            return carry
+
+        lax.fori_loop(0, plane // span, body, 0)
+
+    all_blocks = [(t, h) for t in range(members) for h in range(2)]
+
+    def attended_term(part, levels):
+        left = jnp.concatenate([attended[t, h, part, :] for t, h in all_blocks], axis=1)
+        right = jnp.concatenate(
+            [
+                jnp.concatenate([w_out[level, t, 0 : 2 * hq, :] for t in range(members)], axis=0)
+                for level in levels
+            ],
+            axis=1,
+        )
+        return jnp.dot(left, right, preferred_element_type=f32)
+
+    def pooled_term(part, levels):
+        left = jnp.concatenate([pooled[t, h, part, :] for t, h in all_blocks], axis=1)
+        right = jnp.concatenate(
+            [
+                jnp.concatenate([w_out[level, t, 2 * hq :, :] for t in range(members)], axis=0)
+                for level in levels
+            ],
+            axis=1,
+        )
+        return jnp.dot(left, right, preferred_element_type=f32)
+
+    firsts = (level_of(0), level_of(1))
+    end_events(0, members)
+
+    def first_attended(part):
+        result[part, :] = attended_term(part, firsts)
+
+    by_span(first_attended)
+
+    inner_parts = list(range(1, pooled_parts - 1)) + [0, pooled_parts - 1]
+    for part in inner_parts:
+        pooled_stream.direct(part)
 
     @pl.when(inner)
     def _():
         out_events(members, out_steps)
 
-    lax.fori_loop(0, deep, out_level, 0)
-
-    def results(level, carry):
-        for hop in range(1, 2 * members):
-            result_in(level, hop).wait_recv()
-        return carry
-
-    lax.fori_loop(0, deep, results, 0)
+    for part in inner_parts:
+        pooled_stream.crossed(part)
+    for stream_side in (pooled_stream.near_side, pooled_stream.far_side):
+        pooled_stream.every(stream_side)
+
+    def first_pooled(part):
+        value = (result[part, :] + pooled_term(part, firsts)).astype(bf16)
+        for index, level in enumerate(firsts):
+            rounded[level, part, :] = value[:, index * narrow : (index + 1) * narrow]
+
+    by_span(first_pooled)
+    for level in firsts:
+        send_level(level)
+
+    def middle_level(group, carry):
+        end_events((group - 1) * members, group * members)
+        level = level_of(group)
+
+        def whole_level(part):
+            value = attended_term(part, [level]) + pooled_term(part, [level])
+            rounded[level, part, :] = value.astype(bf16)
+
+        by_span(whole_level)
+        send_level(level)
+        return carry
+
+    lax.fori_loop(2, deep - 1, middle_level, 0)
 
     for ring in (in_ring, pool_ring):
         sends_done(ring)
@@ -1446,12 +1499,42 @@
         out_both(c, sent)
     for c in range(1, members):
         spread(c).wait_send()
-    lax.fori_loop(0, out_steps, out_sent, 0)
     for hop in range(1, members):
         sum_copy(tp, hop).wait_send()
-
     for stream in (token_stream, attend_stream, pooled_stream):
         stream.every(stream.sent)
+
+    level = level_of(deep - 1)
+    for c in range(members):
+        n = (deep - 2) * members + c
+        end_events(n, n + 1)
+        t = (tp - c + members) % members
+
+        def last_level(part, c=c, t=t):
+            left = jnp.concatenate(
+                [attended[t, h, part, :] for h in range(2)]
+                + [pooled[t, h, part, :] for h in range(2)],
+                axis=1,
+            )
+            value = jnp.dot(left, w_out[level, t], preferred_element_type=f32)
+            if c > 0:
+                value = result[part, 0:narrow] + value
+            if c == members - 1:
+                rounded[level, part, :] = value.astype(bf16)
+            else:
+                result[part, 0:narrow] = value
+
+        by_span(last_level)
+    send_level(level)
+
+    def results(level, carry):
+        for hop in range(1, 2 * members):
+            result_in(level, hop).wait_recv()
+        return carry
+
+    lax.fori_loop(0, deep, results, 0)
+
+    lax.fori_loop(0, out_steps, out_sent, 0)
     for index, buffer, size in ((0, band, WINDOW), (2, pool_band, pool_pad)):
 
         @pl.when(has_down)
@@ -1486,15 +1569,15 @@
         pltpu.VMEM((depth, hp), bf16),
         pltpu.VMEM((members, 2 * (hp + hq), narrow), bf16),
         pltpu.VMEM((plane, 2 * hk + hq), f32),
-        pltpu.VMEM((plane, hp), f32),
         pltpu.VMEM((plane + 2 * WINDOW, 2 * hk), bf16),
         pltpu.VMEM((plane + 2 * pool_pad, hp), bf16),
         pltpu.VMEM((plane, 2 * HEAD), f32),
         pltpu.VMEM((plane, 2 * HEAD), f32),
-        pltpu.VMEM((members, 2, plane, hp + hq), bf16),
-        pltpu.VMEM((plane, narrow), f32),
+        pltpu.VMEM((members, 2, plane, hq), bf16),
+        pltpu.VMEM((members, 2, plane, hp), bf16),
+        pltpu.VMEM((plane, 2 * narrow), f32),
         pltpu.VMEM((deep, plane, narrow), bf16),
-        dma((13 + 4 * members,)),
+        dma((11 + 2 * members,)),
         dma((members - 1,)),
         dma((members - 1,)),
         dma((3, count, in_parts)),
@@ -1574,7 +1657,6 @@
     depth, kw = w_key.shape
     qw, pw, width = w_query.shape[1], w_pool.shape[1], w_out_pool.shape[1]
     tables = [jnp.asarray(table) for table in rope_parts(count * rows)]
-    twice = lambda gain: jnp.concatenate([gain, gain]).reshape(1, 2 * HEAD)
     anywhere = pl.BlockSpec(memory_space=pl.ANY)
     in_vmem = pl.BlockSpec(memory_space=pltpu.VMEM)
     sizes = (count, members, rows, features, depth, kw, qw, pw, width)
@@ -1587,6 +1669,7 @@
         and all(size % 256 == 0 for size in (kw, qw, pw))
         and width % (128 * members) == 0
     )
+    as_row = lambda gain: gain.reshape(1, HEAD)
     kernel, scratch = (plane_kernel, plane_scratch) if shared else (layer_kernel, ring_scratch)
     return pl.pallas_call(
         functools.partial(kernel, count, members),
@@ -1606,8 +1689,8 @@
         w_out_pool,
         w_out_attn,
         norm_gain.reshape(members, -1) if shared else norm_gain.reshape(1, -1),
-        twice(query_gain),
-        twice(key_gain),
+        as_row(query_gain),
+        as_row(key_gain),
         *tables,
         sink_logit,
     )

time: 177 us -> 159 us (0.90)
  Pallas kernels: 170 us -> 155 us
    pallas_call x1, Pallas kernels: 170 us -> 155 us  [shards(): pl.pallas_call(functools.partial(kernel, count, members), out_shape=jax.S...]
where the time goes in v3:
time: 159 us
  Pallas kernels  155 us (97%)
  local copies, waits for them, and re-layouts  4.03 us (3%)
    pallas_call x1, Pallas kernels, shards(): pl.pallas_call(functools.partial(kernel, count, members), out_shape=jax.S...  155 us

profile of v3, /device:TPU:1, one launch (start us, length us, event | category | flops | bytes accessed | tf_op | source)
XLA Modules:
  0.0 159.1 jit_solution(10409626424725573469)
XLA Ops:
  0.0 1.3 reshape.9.norm_gain
  1.3 155.1 %shard_map.145 = bf16[192,4096]{1,0:T(8,128)(2,1)} custom-call(bf16[768,1024]{1,0:T(8,128)(2,1)} %tokens.1, bf16[512,512]{1,0:T(8,128)(2,1)} %wq.1, bf16[512,256]{1,0:T(8,128)(2,1)} %wk.1, bf16[512,256]{1,0:T(8,128)(2,1)} %wv.1, bf16[512,256]{1,0:T(8,128)(2,1)} %wp.1, bf16[256,512]{1,0:T(8,128)(2,1)} %wop.1, bf16[512,512]{1,0:T(8,128)(2,1)} %woa.1, ...), custom_call_target="tpu_custom_call" | custom-call | tf_op jit(solution)/shard_map/pallas_call | solution.py:1674
  156.4 2.7 %copy.17 = bf16[192,4096]{1,0:T(8,128)(2,1)} copy(bf16[192,4096]{1,0:T(8,128)(2,1)} %shard_map.145) | data formatting | bytes 3145728

commit v4 on v3

--- a/solution.py
+++ b/solution.py
@@ -19,7 +19,7 @@
 pool_pad = 16
 chunks = 4
 token_chunks = 8
-in_parts = 4
+in_parts = 2
 pooled_parts = 4
 MESH = pl.DeviceIdType.MESH
 f32, bf16 = jnp.float32, jnp.bfloat16
@@ -654,6 +654,15 @@
     wp,
     wop,
     woa,
+    norm_gain_in,
+    query_gain_in,
+    key_gain_in,
+    row_cos_in,
+    row_sin_in,
+    col_cos_in,
+    col_sin_in,
+    sink_in,
+    out,
     norm_gain,
     query_gain,
     key_gain,
@@ -662,7 +671,7 @@
     col_cos,
     col_sin,
     sink,
-    out,
+    small_sem,
     raw,
     sums,
     normed,
@@ -682,20 +691,21 @@
     result,
     rounded,
     load_sem,
-    sum_send,
-    sum_recv,
+    sum_sems,
     in_sems,
     pool_sems,
     out_sems,
     x_sems,
     spread_sems,
     token_sems,
+    token_bulk,
     attend_sems,
+    attend_bulk,
     pooled_sems,
+    pooled_bulk,
     halo_send,
     halo_recv,
-    result_send,
-    result_recv,
+    result_sems,
 ):
     rows, features = tokens.shape
     depth = wk.shape[0]
@@ -709,6 +719,7 @@
     deep = count // 2
     pieces = features // depth
     tiles = rows // WINDOW
+    grid = plane // GRID_W
 
     me, tp = lax.axis_index("sp"), lax.axis_index("tp")
     z, x = me // 2, me % 2
@@ -721,23 +732,42 @@
 
     mine = lambda size: pl.ds(pl.multiple_of(x * size, 128), size)
     other = lambda size: pl.ds(pl.multiple_of((1 - x) * size, 128), size)
-    loads = []
-
-    def load(source, target):
-        loads.append(pltpu.make_async_copy(source, target, load_sem.at[len(loads)]))
-        loads[-1].start()
+
+    def load(group, source, target):
+        pltpu.make_async_copy(source, target, load_sem.at[group]).start()
+
+    def loaded(group, whole):
+        pltpu.make_async_copy(whole, whole, load_sem.at[group]).wait()
 
     for target, pick in ((w_in.at[me], mine), (in_spare, other)):
-        load(wk.at[:, pick(hk)], target.at[:, pl.ds(0, hk)])
-        load(wv.at[:, pick(hk)], target.at[:, pl.ds(hk, hk)])
-        load(wq.at[:, pick(hq)], target.at[:, pl.ds(2 * hk, hq)])
-    load(tokens, raw)
+        load(0, wk.at[:, pick(hk)], target.at[:, pl.ds(0, hk)])
+        load(0, wv.at[:, pick(hk)], target.at[:, pl.ds(hk, hk)])
+        load(0, wq.at[:, pick(hq)], target.at[:, pl.ds(2 * hk, hq)])
+    load(1, tokens, raw)
+    small = [
+        pltpu.make_async_copy(source, target, small_sem.at[index])
+        for index, (source, target) in enumerate(
+            (
+                (norm_gain_in, norm_gain),
+                (query_gain_in, query_gain),
+                (key_gain_in, key_gain),
+                (row_cos_in.at[pl.ds(z * grid, grid), :], row_cos),
+                (row_sin_in.at[pl.ds(z * grid, grid), :], row_sin),
+                (col_cos_in, col_cos),
+                (col_sin_in, col_sin),
+                (sink_in, sink),
+            )
+        )
+    ]
+    for copy in small:
+        copy.start()
     for target, pick in ((w_pool.at[me], mine), (pool_spare, other)):
-        load(wp.at[:, pick(hp)], target)
+        load(2, wp.at[:, pick(hp)], target)
     strip = lambda t: pl.ds(pl.multiple_of(t * narrow, narrow), narrow)
-    for target, t in [(w_out.at[z, tp], tp)] + [(out_spare.at[t], t) for t in range(members)]:
-        load(woa.at[:, strip(t)], target.at[pl.ds(0, 2 * hq), :])
-        load(wop.at[:, strip(t)], target.at[pl.ds(2 * hq, 2 * hp), :])
+    strips = [(3, w_out.at[z, tp], tp)] + [(4, out_spare.at[t], t) for t in range(members)]
+    for group, target, t in strips:
+        load(group, woa.at[:, strip(t)], target.at[pl.ds(0, 2 * hq), :])
+        load(group, wop.at[:, strip(t)], target.at[pl.ds(2 * hq, 2 * hp), :])
 
     barrier = pltpu.get_barrier_semaphore()
     greeted = [(up, tp), (down, tp), (me_x, tp)]
@@ -765,32 +795,31 @@
         return view
 
     in_ring = (w_in, in_spare, in_sems, 0, in_parts, by_rows(in_parts))
-    pool_ring = (w_pool, pool_spare, pool_sems, in_parts, 1, by_rows(1))
-    def z_copy(ring, way, source, c):
+    pool_ring = (w_pool, pool_spare, pool_sems, 1, 1, by_rows(1))
+    def z_copy(ring, way, source, c, own=False):
         buffer, _, sems, _, _, view = ring
         part = view(buffer.at[source], c)
-        return remote(
-            part, part, sems.at[way, source, c], sems.at[2, source, c], ((up, down)[way], tp)
-        )
+        send = sems.at[int(own and way == 1), source, c]
+        return remote(part, part, send, sems.at[1, source, c], ((up, down)[way], tp))
 
     def x_copy(ring, source, c):
         buffer, spare, sems, first, _, view = ring
         return remote(
             view(spare, c),
             view(buffer.at[source], c),
-            x_sems.at[first + c],
-            sems.at[2, source, c],
+            x_sems.at[first],
+            sems.at[1, source, c],
             (me_x, tp),
         )
 
     def both_ways(ring, source, c, act):
         @pl.when(has_up)
         def _():
-            act(z_copy(ring, 0, source, c))
+            act(z_copy(ring, 0, source, c, own=True))
 
         @pl.when(has_down)
         def _():
-            act(z_copy(ring, 1, source, c))
+            act(z_copy(ring, 1, source, c, own=True))
 
     start = lambda copy: copy.start()
     sent = lambda copy: copy.wait_send()
@@ -844,11 +873,14 @@
     def all_events(ring):
         return (deep - 1) * 2 * ring[4]
 
+    def bulk(whole, sem):
+        return remote(whole, whole, sem, sem, (me_x, tp))
+
     def sends_done(ring):
+        bulk(ring[1], x_sems.at[ring[3]]).wait_send()
         for c in range(ring[4]):
             both_ways(ring, me, c, sent)
             both_ways(ring, me_x, c, sent)
-            x_copy(ring, me, c).wait_send()
 
         def body(n, carry):
             (is_low, low), (is_high, high), c = passing(ring, n)
@@ -865,18 +897,18 @@
 
         lax.fori_loop(0, all_events(ring), body, 0)
 
-    def out_copy(way, level, c):
+    def out_copy(way, level, c, own=False):
         part = w_out.at[level, (tp - c + members) % members]
-        device = ((up, down)[way], tp)
-        return remote(part, part, out_sems.at[way, level, c], out_sems.at[2, level, c], device)
+        send = out_sems.at[int(own and way == 1), level, c]
+        return remote(part, part, send, out_sems.at[1, level, c], ((up, down)[way], tp))
 
     def spread(c):
         target = (tp + c) % members
         return remote(
             out_spare.at[target],
             w_out.at[z, tp],
-            spread_sems.at[c],
-            out_sems.at[2, z, c],
+            spread_sems.at[0],
+            out_sems.at[1, z, c],
             (me, target),
         )
 
@@ -885,19 +917,19 @@
         return remote(
             out_spare.at[owner],
             w_out.at[z, owner],
-            spread_sems.at[c],
-            out_sems.at[2, z, c],
+            spread_sems.at[0],
+            out_sems.at[1, z, c],
             (me, owner),
         )
 
     def out_both(c, act):
         @pl.when(has_up)
         def _():
-            act(out_copy(0, z, c))
+            act(out_copy(0, z, c, own=True))
 
         @pl.when(has_down)
         def _():
-            act(out_copy(1, z, c))
+            act(out_copy(1, z, c, own=True))
 
     def out_event(n):
         step, c = n // members + 1, n % members
@@ -940,13 +972,14 @@
 
         return carry
 
-    for copy in loads[:6]:
-        copy.wait()
+    loaded(0, w_in.at[pl.ds(0, 2)])
     for c in range(in_parts):
         x_copy(in_ring, me, c).start()
         both_ways(in_ring, me, c, start)
 
-    loads[6].wait()
+    loaded(1, raw)
+    for copy in small:
+        copy.wait()
     sums[tp] = jnp.zeros_like(sums[tp])
     for i in range(tiles):
         block = raw[i * WINDOW : (i + 1) * WINDOW, :].astype(f32)
@@ -959,42 +992,40 @@
         return remote(
             sums.at[owner],
             sums.at[owner],
-            sum_send.at[hop - 1],
-            sum_recv.at[hop - 1],
+            sum_sems.at[0],
+            sum_sems.at[1],
             (me, target),
         )
 
     for hop in range(1, members):
         sum_copy(tp, hop).start()
-    for g in range(plane // GRID_W):
-        spot = pl.ds(z * (plane // GRID_W) + g, 1)
+    for g in range(grid):
         grid_rows = pl.ds(g * GRID_W, GRID_W)
-        cosines[grid_rows, :] = col_cos[...] + row_cos[spot, :]
-        sines[grid_rows, :] = col_sin[...] + row_sin[spot, :]
-    for hop in range(1, members):
-        sum_copy((tp - hop + members) % members, hop).wait_recv()
+        cosines[grid_rows, :] = col_cos[...] + row_cos[g : g + 1, :]
+        sines[grid_rows, :] = col_sin[...] + row_sin[g : g + 1, :]
+    bulk(sums.at[pl.ds(0, members - 1)], sum_sems.at[1]).wait_recv()
     squares = sums[0]
     for t in range(1, members):
         squares = squares + sums[t]
     scales = lax.rsqrt(squares / (members * features) + eps)
 
     class Stream:
-        def __init__(self, view, sems, by_x):
-            self.view, self.sems, self.by_x = view, sems, by_x
-
-        def copy(self, base, count_of, slot, side, owner, j, device):
+        def __init__(self, view, all_sent, side, sems, bulk_sems, by_x):
+            self.view, self.all_sent, self.side = view, all_sent, side
+            self.sems, self.bulk_sems, self.by_x = sems, bulk_sems, by_x
+
+        def copy(self, recv, side, owner, j, device):
             part = self.view(side, owner, j)
-            send, recv = self.sems.at[base + slot, j], self.sems.at[base + count_of + slot, j]
-            return remote(part, part, send, recv, device)
+            return remote(part, part, self.bulk_sems.at[0], recv, device)
 
         def over_x(self, slot, side, owner, j):
-            return self.copy(0, 2, slot, side, owner, j, (me_x, tp))
+            return self.copy(self.sems.at[2 * slot, j], side, owner, j, (me_x, tp))
 
         def over_y(self, slot, side, owner, j):
-            return self.copy(4, 2, slot, side, owner, j, (me, tp_y))
+            return self.copy(self.sems.at[1 + slot, j], side, owner, j, (me, tp_y))
 
         def over_core(self, slot, side, owner, j):
-            return self.copy(8, 4, slot, side, owner, j, (me, tp_c))
+            return self.copy(self.bulk_sems.at[1 + slot % 2], side, owner, j, (me, tp_c))
 
         def start(self, j):
             self.over_y(0, x, tp, j).start()
@@ -1027,29 +1058,14 @@
 
             self.over_core(3, 1 - x, tp_y, j).start()
 
-        def near_side(self, j):
-            self.over_core(0, x, tp_c, j).wait_recv()
-            self.over_core(2, x, tp_yc, j).wait_recv()
-
-        def far_side(self, j):
-            self.over_core(1, 1 - x, tp_c, j).wait_recv()
-            self.over_core(3, 1 - x, tp_yc, j).wait_recv()
-
-        def sent(self, j):
-            self.over_y(0, x, tp, j).wait_send()
-            self.over_x(0, x, tp, j).wait_send()
-            self.over_core(0, x, tp, j).wait_send()
-            self.over_core(1, 1 - x, tp, j).wait_send()
-            self.over_core(2, x, tp_y, j).wait_send()
-            self.over_core(3, 1 - x, tp_y, j).wait_send()
-
-            @pl.when(self.by_x(j))
-            def _():
-                self.over_x(1, x, tp_y, j).wait_send()
-
-            @pl.when(jnp.logical_not(self.by_x(j)))
-            def _():
-                self.over_y(1, 1 - x, tp, j).wait_send()
+        def near_side(self):
+            bulk(self.side, self.bulk_sems.at[1]).wait_recv()
+
+        def far_side(self):
+            bulk(self.side, self.bulk_sems.at[2]).wait_recv()
+
+        def sent(self):
+            bulk(self.all_sent, self.bulk_sems.at[0]).wait_send()
 
         def every(self, act):
             def body(j, carry):
@@ -1070,17 +1086,37 @@
     def pooled_view(side, owner, j):
         return pooled.at[owner, side, block_rows(j, plane // pooled_parts), :]
 
-    token_stream = Stream(token_view, token_sems, lambda j: j % 3 == 0)
-    attend_stream = Stream(attend_view, attend_sems, lambda j: j % 2 == 0)
-    pooled_stream = Stream(pooled_view, pooled_sems, lambda j: j % 2 == 0)
-
-    gains = norm_gain[pl.ds(tp, 1), :]
+    most = lambda size: pl.ds(0, size * (2 * members - 1) // (2 * members))
+    token_stream = Stream(
+        token_view,
+        normed.at[:, :, most(rows), :],
+        normed.at[0, pl.ds(0, count // 2)],
+        token_sems,
+        token_bulk,
+        lambda j: j % 3 == 0,
+    )
+    attend_stream, pooled_stream = [
+        Stream(
+            view,
+            buffer.at[:, :, most(plane), :],
+            buffer.at[0],
+            sems,
+            bulk_sems,
+            lambda j: j % 2 == 0,
+        )
+        for view, buffer, sems, bulk_sems in (
+            (attend_view, attended, attend_sems, attend_bulk),
+            (pooled_view, pooled, pooled_sems, pooled_bulk),
+        )
+    ]
+
     for i in range(tiles):
         here = slice(i * WINDOW, (i + 1) * WINDOW)
         scale = jnp.transpose(jnp.broadcast_to(scales[i : i + 1, :], (WINDOW, WINDOW)))
         for first in range(0, features, WINDOW):
             block = raw[here, first : first + WINDOW].astype(f32)
-            value = (block * scale * gains[:, first : first + WINDOW]).astype(bf16)
+            gain = norm_gain[:, pl.ds(pl.multiple_of(tp * features + first, WINDOW), WINDOW)]
+            value = (block * scale * gain).astype(bf16)
             inside = first % depth
             normed[x, tp * pieces + first // depth, here, inside : inside + WINDOW] = value
         token_stream.start(i)
@@ -1096,12 +1132,13 @@
         return carry
 
     lax.fori_loop(0, tiles, direct, 0)
-    for copy in loads[7:]:
-        copy.wait()
+    loaded(2, w_pool.at[pl.ds(0, 2)])
+    loaded(3, w_out.at[0, 0])
+    loaded(4, out_spare)
     side_out(pool_ring)
     for c in range(1, members):
         spread(c).start()
-    token_stream.every(token_stream.near_side)
+    token_stream.near_side()
 
     tile_rows = 256 if rows % 256 == 0 else 128
     per_side = rows // tile_rows
@@ -1151,7 +1188,7 @@
     lax.fori_loop(0, tiles, crossed, 0)
     own_out(pool_ring)
     side_in(pool_ring)
-    token_stream.every(token_stream.far_side)
+    token_stream.far_side()
     project(total, w_in, z, 1 - x, first=True)
 
     @pl.when(inner)
@@ -1364,8 +1401,8 @@
         out_events(members - 1, members)
 
     attend_stream.every(attend_stream.crossed)
-    for stream_side in (attend_stream.near_side, attend_stream.far_side):
-        attend_stream.every(stream_side)
+    attend_stream.near_side()
+    attend_stream.far_side()
 
     def level_of(group):
         paired = jnp.minimum(z, deep - 1 - z)
@@ -1385,26 +1422,16 @@
         return remote(
             rounded.at[level, pl.ds(pl.multiple_of(target * share, 16), share), :],
             out.at[:, columns_of(level, x, tp)],
-            result_send.at[level, hop],
-            result_recv.at[level, hop],
+            result_sems.at[0, level],
+            result_sems.at[1, level],
             (z * 2 + target // members, target % members),
-        )
-
-    def result_in(level, hop):
-        source = (here - hop + 2 * members) % (2 * members)
-        return remote(
-            rounded.at[level, pl.ds(0, share), :],
-            out.at[:, columns_of(level, source // members, source % members)],
-            result_send.at[level, hop],
-            result_recv.at[level, hop],
-            (z * 2 + source // members, source % members),
         )
 
     def result_own(level):
         return pltpu.make_async_copy(
             rounded.at[level, pl.ds(pl.multiple_of(here * share, 16), share), :],
             out.at[:, columns_of(level, x, tp)],
-            result_send.at[level, 0],
+            result_sems.at[2, level],
         )
 
     def send_level(level):
@@ -1467,8 +1494,8 @@
 
     for part in inner_parts:
         pooled_stream.crossed(part)
-    for stream_side in (pooled_stream.near_side, pooled_stream.far_side):
-        pooled_stream.every(stream_side)
+    pooled_stream.near_side()
+    pooled_stream.far_side()
 
     def first_pooled(part):
         value = (result[part, :] + pooled_term(part, firsts)).astype(bf16)
@@ -1497,12 +1524,10 @@
         sends_done(ring)
     for c in range(members):
         out_both(c, sent)
-    for c in range(1, members):
-        spread(c).wait_send()
-    for hop in range(1, members):
-        sum_copy(tp, hop).wait_send()
+    bulk(out_spare.at[pl.ds(0, members - 1)], spread_sems.at[0]).wait_send()
+    bulk(sums.at[pl.ds(0, members - 1)], sum_sems.at[0]).wait_send()
     for stream in (token_stream, attend_stream, pooled_stream):
-        stream.every(stream.sent)
+        stream.sent()
 
     level = level_of(deep - 1)
     for c in range(members):
@@ -1527,9 +1552,10 @@
         by_span(last_level)
     send_level(level)
 
+    arrivals = out.at[:, pl.ds(0, (2 * members - 1) * narrow)]
+
     def results(level, carry):
-        for hop in range(1, 2 * members):
-            result_in(level, hop).wait_recv()
+        bulk(arrivals, result_sems.at[1, level]).wait_recv()
         return carry
 
     lax.fori_loop(0, deep, results, 0)
@@ -1546,8 +1572,7 @@
             halo(index + 1, buffer, size, True).wait_send()
 
     def results_sent(level, carry):
-        for hop in range(1, 2 * members):
-            result_copy(level, hop).wait_send()
+        bulk(rounded.at[level, most(plane), :], result_sems.at[0, level]).wait_send()
         result_own(level).wait()
         return carry
 
@@ -1559,6 +1584,15 @@
     narrow, plane, deep, tiles = width // members, 2 * rows, count // 2, rows // WINDOW
     dma = pltpu.SemaphoreType.DMA
     return [
+        pltpu.VMEM((1, members * features), f32),
+        pltpu.VMEM((1, HEAD), f32),
+        pltpu.VMEM((1, HEAD), f32),
+        pltpu.VMEM((plane // GRID_W, 2 * HEAD), f32),
+        pltpu.VMEM((plane // GRID_W, 2 * HEAD), f32),
+        pltpu.VMEM((GRID_W, 2 * HEAD), f32),
+        pltpu.VMEM((GRID_W, 2 * HEAD), f32),
+        pltpu.SMEM((2 * hq // HEAD,), f32),
+        dma((8,)),
         pltpu.VMEM((rows, features), bf16),
         pltpu.VMEM((members, -(-tiles // 8) * 8, WINDOW), f32),
         pltpu.VMEM((2, count, rows, depth), bf16),
@@ -1577,21 +1611,22 @@
         pltpu.VMEM((members, 2, plane, hp), bf16),
         pltpu.VMEM((plane, 2 * narrow), f32),
         pltpu.VMEM((deep, plane, narrow), bf16),
-        dma((11 + 2 * members,)),
-        dma((members - 1,)),
-        dma((members - 1,)),
-        dma((3, count, in_parts)),
-        dma((3, count, 1)),
-        dma((3, deep, members)),
-        dma((in_parts + 1,)),
-        dma((members,)),
-        dma((16, tiles)),
-        dma((16, 2 * tiles)),
-        dma((16, pooled_parts)),
+        dma((5,)),
+        dma((2,)),
+        dma((2, count, in_parts)),
+        dma((2, count, 1)),
+        dma((2, deep, members)),
+        dma((2,)),
+        dma((1,)),
+        dma((3, tiles)),
+        dma((3,)),
+        dma((3, 2 * tiles)),
+        dma((3,)),
+        dma((3, pooled_parts)),
+        dma((3,)),
         dma((4,)),
         dma((4,)),
-        dma((deep, 2 * members)),
-        dma((deep, 2 * members)),
+        dma((3, deep)),
     ]
 
 
@@ -1669,18 +1704,13 @@
         and all(size % 256 == 0 for size in (kw, qw, pw))
         and width % (128 * members) == 0
     )
+    grant = (46 if shared else 60) * 1024 * 1024
+    specs = [anywhere] * 7 + [in_vmem] * 7 + [pl.BlockSpec(memory_space=pltpu.SMEM)]
+    if shared:
+        specs = [pl.BlockSpec(memory_space=pltpu.HBM)] * 15
     as_row = lambda gain: gain.reshape(1, HEAD)
     kernel, scratch = (plane_kernel, plane_scratch) if shared else (layer_kernel, ring_scratch)
-    return pl.pallas_call(
-        functools.partial(kernel, count, members),
-        out_shape=jax.ShapeDtypeStruct((rows // members, count * width), bf16),
-        in_specs=[anywhere] * 7 + [in_vmem] * 7 + [pl.BlockSpec(memory_space=pltpu.SMEM)],
-        out_specs=anywhere,
-        scratch_shapes=scratch(*sizes),
-        compiler_params=pltpu.CompilerParams(
-            collective_id=0, has_side_effects=True, vmem_limit_bytes=62 * 1024 * 1024
-        ),
-    )(
+    operands = (
         tokens,
         w_query,
         w_key,
@@ -1688,12 +1718,27 @@
         w_pool,
         w_out_pool,
         w_out_attn,
-        norm_gain.reshape(members, -1) if shared else norm_gain.reshape(1, -1),
+        norm_gain.reshape(1, -1),
         as_row(query_gain),
         as_row(key_gain),
         *tables,
         sink_logit,
     )
+    shape = (rows // members, count * width)
+    result = jax.ShapeDtypeStruct(shape, bf16)
+    if shared:
+        operands = [pltpu.with_memory_space_constraint(each, pltpu.HBM) for each in operands]
+        result = pltpu.VMEM(shape, bf16)
+    return pl.pallas_call(
+        functools.partial(kernel, count, members),
+        out_shape=result,
+        in_specs=specs,
+        out_specs=anywhere,
+        scratch_shapes=scratch(*sizes),
+        compiler_params=pltpu.CompilerParams(
+            collective_id=0, has_side_effects=True, vmem_limit_bytes=grant
+        ),
+    )(*operands)
 
 
 def solution(mesh):

time: 159 us -> 151 us (0.950)
  Pallas kernels: 155 us -> 150 us
  local copies, waits for them, and re-layouts: 4.03 us -> 1.15 us
    pallas_call x1, Pallas kernels: 155 us -> 150 us  [shards(): pl.pallas_call(functools.partial(kernel, count, members), out_shape=resul...]
where the time goes in v4:
time: 151 us
  Pallas kernels  150 us (99%)
    pallas_call x1, Pallas kernels, shards(): pl.pallas_call(functools.partial(kernel, count, members), out_shape=resul...  150 us

profile of v4, /device:TPU:1, one launch (start us, length us, event | category | flops | bytes accessed | tf_op | source)
XLA Modules:
  0.0 151.2 jit_solution(5031798587438480022)
XLA Ops:
  0.0 150.1 %shard_map.145 = bf16[192,4096]{1,0:T(8,128)(2,1)S(1)} custom-call(bf16[768,1024]{1,0:T(8,128)(2,1)} %tokens.1, bf16[512,512]{1,0:T(8,128)(2,1)} %wq.1, bf16[512,256]{1,0:T(8,128)(2,1)} %wk.1, bf16[512,256]{1,0:T(8,128)(2,1)} %wv.1, bf16[512,256]{1,0:T(8,128)(2,1)} %wp.1, bf16[256,512]{1,0:T(8,128)(2,1)} %wop.1, bf16[512,512]{1,0:T(8,128)(2,1)} %woa.1, ...), custom_call_target="tpu_custom_call" | custom-call | tf_op jit(solution)/shard_map/pallas_call | solution.py:1732
  150.1 1.1 copy.17

commit v5 on v4

--- a/solution.py
+++ b/solution.py
@@ -696,6 +696,7 @@
     pool_sems,
     out_sems,
     x_sems,
+    ring_sems,
     spread_sems,
     token_sems,
     token_bulk,
@@ -796,11 +797,11 @@
 
     in_ring = (w_in, in_spare, in_sems, 0, in_parts, by_rows(in_parts))
     pool_ring = (w_pool, pool_spare, pool_sems, 1, 1, by_rows(1))
-    def z_copy(ring, way, source, c, own=False):
+    def z_copy(ring, way, source, c):
         buffer, _, sems, _, _, view = ring
         part = view(buffer.at[source], c)
-        send = sems.at[int(own and way == 1), source, c]
-        return remote(part, part, send, sems.at[1, source, c], ((up, down)[way], tp))
+        send = ring_sems.at[ring[3], way]
+        return remote(part, part, send, sems.at[source, c], ((up, down)[way], tp))
 
     def x_copy(ring, source, c):
         buffer, spare, sems, first, _, view = ring
@@ -808,21 +809,20 @@
             view(spare, c),
             view(buffer.at[source], c),
             x_sems.at[first],
-            sems.at[1, source, c],
+            sems.at[source, c],
             (me_x, tp),
         )
 
     def both_ways(ring, source, c, act):
         @pl.when(has_up)
         def _():
-            act(z_copy(ring, 0, source, c, own=True))
+            act(z_copy(ring, 0, source, c))
 
         @pl.when(has_down)
         def _():
-            act(z_copy(ring, 1, source, c, own=True))
+            act(z_copy(ring, 1, source, c))
 
     start = lambda copy: copy.start()
-    sent = lambda copy: copy.wait_send()
 
     def own_out(ring):
         for c in range(ring[4]):
@@ -876,31 +876,22 @@
     def bulk(whole, sem):
         return remote(whole, whole, sem, sem, (me_x, tp))
 
-    def sends_done(ring):
-        bulk(ring[1], x_sems.at[ring[3]]).wait_send()
-        for c in range(ring[4]):
-            both_ways(ring, me, c, sent)
-            both_ways(ring, me_x, c, sent)
-
-        def body(n, carry):
-            (is_low, low), (is_high, high), c = passing(ring, n)
-
-            @pl.when(is_low & has_up)
-            def _():
-                z_copy(ring, 0, low, c).wait_send()
-
-            @pl.when(is_high & has_down)
-            def _():
-                z_copy(ring, 1, high, c).wait_send()
-
-            return carry
-
-        lax.fori_loop(0, all_events(ring), body, 0)
-
-    def out_copy(way, level, c, own=False):
+    def sends_done(buffer, sem, each):
+        for level in range(deep):
+
+            @pl.when(z == level)
+            def _(level=level):
+                if level < deep - 1:
+                    whole = buffer.at[pl.ds(0, (level + 1) * each)]
+                    bulk(whole, ring_sems.at[sem, 0]).wait_send()
+                if level > 0:
+                    whole = buffer.at[pl.ds(0, (deep - level) * each)]
+                    bulk(whole, ring_sems.at[sem, 1]).wait_send()
+
+    def out_copy(way, level, c):
         part = w_out.at[level, (tp - c + members) % members]
-        send = out_sems.at[int(own and way == 1), level, c]
-        return remote(part, part, send, out_sems.at[1, level, c], ((up, down)[way], tp))
+        send = ring_sems.at[2, way]
+        return remote(part, part, send, out_sems.at[level, c], ((up, down)[way], tp))
 
     def spread(c):
         target = (tp + c) % members
@@ -908,7 +899,7 @@
             out_spare.at[target],
             w_out.at[z, tp],
             spread_sems.at[0],
-            out_sems.at[1, z, c],
+            out_sems.at[z, c],
             (me, target),
         )
 
@@ -918,18 +909,18 @@
             out_spare.at[owner],
             w_out.at[z, owner],
             spread_sems.at[0],
-            out_sems.at[1, z, c],
+            out_sems.at[z, c],
             (me, owner),
         )
 
     def out_both(c, act):
         @pl.when(has_up)
         def _():
-            act(out_copy(0, z, c, own=True))
+            act(out_copy(0, z, c))
 
         @pl.when(has_down)
         def _():
-            act(out_copy(1, z, c, own=True))
+            act(out_copy(1, z, c))
 
     def out_event(n):
         step, c = n // members + 1, n % members
@@ -957,20 +948,6 @@
             return carry
 
         lax.fori_loop(first, last, body, 0)
-
-    def out_sent(n, carry):
-        step, c = n // members + 1, n % members
-        low, high = z - step, z + step
-
-        @pl.when((low >= 0) & has_up)
-        def _():
-            out_copy(0, low, c).wait_send()
-
-        @pl.when((high < deep) & has_down)
-        def _():
-            out_copy(1, high, c).wait_send()
-
-        return carry
 
     loaded(0, w_in.at[pl.ds(0, 2)])
     for c in range(in_parts):
@@ -1417,14 +1394,14 @@
         first = (level * 2 + side) * width + t * narrow
         return pl.ds(pl.multiple_of(first, narrow), narrow)
 
-    def result_copy(level, hop):
-        target = (here + hop) % (2 * members)
+    def result_copy(level, side, t):
+        first = pl.multiple_of((side * members + t) * share, 16)
         return remote(
-            rounded.at[level, pl.ds(pl.multiple_of(target * share, 16), share), :],
+            rounded.at[level, pl.ds(first, share), :],
             out.at[:, columns_of(level, x, tp)],
             result_sems.at[0, level],
             result_sems.at[1, level],
-            (z * 2 + target // members, target % members),
+            (z * 2 + side, t),
         )
 
     def result_own(level):
@@ -1434,10 +1411,18 @@
             result_sems.at[2, level],
         )
 
+    def send_far(level):
+        for hop in range(members):
+            result_copy(level, 1 - x, (tp + hop) % members).start()
+
+    def send_near(level):
+        for hop in range(1, members):
+            result_copy(level, x, (tp + hop) % members).start()
+        result_own(level).start()
+
     def send_level(level):
-        for hop in range(1, 2 * members):
-            result_copy(level, hop).start()
-        result_own(level).start()
+        send_far(level)
+        send_near(level)
 
     span = 2 * tile_rows if plane % (2 * tile_rows) == 0 else tile_rows
     ends_event = lambda n: jnp.where(inner, out_steps, n)
@@ -1521,9 +1506,8 @@
     lax.fori_loop(2, deep - 1, middle_level, 0)
 
     for ring in (in_ring, pool_ring):
-        sends_done(ring)
-    for c in range(members):
-        out_both(c, sent)
+        bulk(ring[1], x_sems.at[ring[3]]).wait_send()
+        sends_done(ring[0], ring[3], 2)
     bulk(out_spare.at[pl.ds(0, members - 1)], spread_sems.at[0]).wait_send()
     bulk(sums.at[pl.ds(0, members - 1)], sum_sems.at[0]).wait_send()
     for stream in (token_stream, attend_stream, pooled_stream):
@@ -1549,8 +1533,14 @@
             else:
                 result[part, 0:narrow] = value
 
-        by_span(last_level)
-    send_level(level)
+        if c < members - 1:
+            by_span(last_level)
+            continue
+        for side, send in ((1 - x, send_far), (x, send_near)):
+            for start_row in range(0, rows, rows // 2):
+                first = pl.multiple_of(side * rows + start_row, rows // 2)
+                last_level(pl.ds(first, rows // 2))
+            send(level)
 
     arrivals = out.at[:, pl.ds(0, (2 * members - 1) * narrow)]
 
@@ -1560,7 +1550,7 @@
 
     lax.fori_loop(0, deep, results, 0)
 
-    lax.fori_loop(0, out_steps, out_sent, 0)
+    sends_done(w_out, 2, 1)
     for index, buffer, size in ((0, band, WINDOW), (2, pool_band, pool_pad)):
 
         @pl.when(has_down)
@@ -1613,10 +1603,11 @@
         pltpu.VMEM((deep, plane, narrow), bf16),
         dma((5,)),
         dma((2,)),
-        dma((2, count, in_parts)),
-        dma((2, count, 1)),
-        dma((2, deep, members)),
+        dma((count, in_parts)),
+        dma((count, 1)),
+        dma((deep, members)),
         dma((2,)),
+        dma((3, 2)),
         dma((1,)),
         dma((3, tiles)),
         dma((3,)),

time: 151 us -> 151 us (level)
  no operation moved by 1% of the time
where the time goes in v5:
time: 151 us
  Pallas kernels  150 us (99%)
    pallas_call x1, Pallas kernels, shards(): pl.pallas_call(functools.partial(kernel, count, members), out_shape=resul...  150 us

profile of v5, /device:TPU:1, one launch (start us, length us, event | category | flops | bytes accessed | tf_op | source)
XLA Modules:
  0.0 150.8 jit_solution(445379803521994982)
XLA Ops:
  0.0 149.6 %shard_map.145 = bf16[192,4096]{1,0:T(8,128)(2,1)S(1)} custom-call(bf16[768,1024]{1,0:T(8,128)(2,1)} %tokens.1, bf16[512,512]{1,0:T(8,128)(2,1)} %wq.1, bf16[512,256]{1,0:T(8,128)(2,1)} %wk.1, bf16[512,256]{1,0:T(8,128)(2,1)} %wv.1, bf16[512,256]{1,0:T(8,128)(2,1)} %wp.1, bf16[256,512]{1,0:T(8,128)(2,1)} %wop.1, bf16[512,512]{1,0:T(8,128)(2,1)} %woa.1, ...), custom_call_target="tpu_custom_call" | custom-call | tf_op jit(solution)/shard_map/pallas_call | solution.py:1723
  149.7 1.1 copy.17

commit v6 on v5

--- a/solution.py
+++ b/solution.py
@@ -707,6 +707,7 @@
     halo_send,
     halo_recv,
     result_sems,
+    go_sem,
 ):
     rows, features = tokens.shape
     depth = wk.shape[0]
@@ -771,9 +772,7 @@
         load(group, wop.at[:, strip(t)], target.at[pl.ds(2 * hq, 2 * hp), :])
 
     barrier = pltpu.get_barrier_semaphore()
-    greeted = [(up, tp), (down, tp), (me_x, tp)]
-    for t in (tp_y, tp_c, tp_yc):
-        greeted += [(me, t), (me_x, t)]
+    greeted = [(up, tp), (down, tp), (me_x, tp), (me, tp_y), (me, tp_c), (me, tp_yc)]
     for device in greeted:
         pl.semaphore_signal(barrier, inc=1, device_id=device, device_id_type=MESH)
     pl.semaphore_wait(barrier, len(greeted))
@@ -922,6 +921,21 @@
         def _():
             act(out_copy(1, z, c))
 
+    skewed = deep >= 4
+    late_up = skewed & (core == 1) & (z == deep - 2)
+    late_down = skewed & (core == 1) & (z == 1)
+
+    def late_copies(act):
+        @pl.when(late_up)
+        def _():
+            for c in range(members):
+                act(out_copy(0, 0, c))
+
+        @pl.when(late_down)
+        def _():
+            for c in range(members):
+                act(out_copy(1, deep - 1, c))
+
     def out_event(n):
         step, c = n // members + 1, n % members
         low, high = z - step, z + step
@@ -930,7 +944,7 @@
         def _():
             out_copy(0, low, c).wait_recv()
 
-            @pl.when(has_up)
+            @pl.when(has_up & jnp.logical_not(late_up & (low == 0)))
             def _():
                 out_copy(0, low, c).start()
 
@@ -938,7 +952,7 @@
         def _():
             out_copy(1, high, c).wait_recv()
 
-            @pl.when(has_down)
+            @pl.when(has_down & jnp.logical_not(late_down & (high == deep - 1)))
             def _():
                 out_copy(1, high, c).start()
 
@@ -987,7 +1001,8 @@
     scales = lax.rsqrt(squares / (members * features) + eps)
 
     class Stream:
-        def __init__(self, view, all_sent, side, sems, bulk_sems, by_x):
+        def __init__(self, view, all_sent, side, sems, bulk_sems, by_x, pair=None):
+            self.pair, self.crossing = pair, 1 if pair else 2
             self.view, self.all_sent, self.side = view, all_sent, side
             self.sems, self.bulk_sems, self.by_x = sems, bulk_sems, by_x
 
@@ -996,10 +1011,11 @@
             return remote(part, part, self.bulk_sems.at[0], recv, device)
 
         def over_x(self, slot, side, owner, j):
-            return self.copy(self.sems.at[2 * slot, j], side, owner, j, (me_x, tp))
+            return self.copy(self.sems.at[slot * self.crossing, j], side, owner, j, (me_x, tp))
 
         def over_y(self, slot, side, owner, j):
-            return self.copy(self.sems.at[1 + slot, j], side, owner, j, (me, tp_y))
+            index = slot * self.crossing if self.pair or slot else 1
+            return self.copy(self.sems.at[index, j], side, owner, j, (me, tp_y))
 
         def over_core(self, slot, side, owner, j):
             return self.copy(self.bulk_sems.at[1 + slot % 2], side, owner, j, (me, tp_c))
@@ -1010,14 +1026,18 @@
             self.over_core(0, x, tp, j).start()
 
         def direct(self, j):
-            self.over_y(0, x, tp_y, j).wait_recv()
+            if self.pair:
+                bulk(self.pair(j), self.sems.at[0, j]).wait_recv()
+            else:
+                self.over_y(0, x, tp_y, j).wait_recv()
             self.over_core(2, x, tp_y, j).start()
 
             @pl.when(self.by_x(j))
             def _():
                 self.over_x(1, x, tp_y, j).start()
 
-            self.over_x(0, 1 - x, tp, j).wait_recv()
+            if not self.pair:
+                self.over_x(0, 1 - x, tp, j).wait_recv()
             self.over_core(1, 1 - x, tp, j).start()
 
             @pl.when(jnp.logical_not(self.by_x(j)))
@@ -1080,10 +1100,11 @@
             sems,
             bulk_sems,
             lambda j: j % 2 == 0,
-        )
-        for view, buffer, sems, bulk_sems in (
-            (attend_view, attended, attend_sems, attend_bulk),
-            (pooled_view, pooled, pooled_sems, pooled_bulk),
+            lambda j, buffer=buffer, size=size: buffer.at[0, :, block_rows(j, size), :],
+        )
+        for view, buffer, sems, bulk_sems, size in (
+            (attend_view, attended, attend_sems, attend_bulk, WINDOW),
+            (pooled_view, pooled, pooled_sems, pooled_bulk, plane // pooled_parts),
         )
     ]
 
@@ -1399,8 +1420,8 @@
         return remote(
             rounded.at[level, pl.ds(first, share), :],
             out.at[:, columns_of(level, x, tp)],
-            result_sems.at[0, level],
-            result_sems.at[1, level],
+            result_sems.at[0],
+            result_sems.at[1],
             (z * 2 + side, t),
         )
 
@@ -1408,16 +1429,16 @@
         return pltpu.make_async_copy(
             rounded.at[level, pl.ds(pl.multiple_of(here * share, 16), share), :],
             out.at[:, columns_of(level, x, tp)],
-            result_sems.at[2, level],
+            result_sems.at[2],
         )
 
     def send_far(level):
-        for hop in range(members):
-            result_copy(level, 1 - x, (tp + hop) % members).start()
+        for t in (tp_y, tp_yc, tp, tp_c):
+            result_copy(level, 1 - x, t).start()
 
     def send_near(level):
-        for hop in range(1, members):
-            result_copy(level, x, (tp + hop) % members).start()
+        for t in (tp_y, tp_yc, tp_c):
+            result_copy(level, x, t).start()
         result_own(level).start()
 
     def send_level(level):
@@ -1512,6 +1533,11 @@
     bulk(sums.at[pl.ds(0, members - 1)], sum_sems.at[0]).wait_send()
     for stream in (token_stream, attend_stream, pooled_stream):
         stream.sent()
+
+    @pl.when(late_up | late_down)
+    def _():
+        pl.semaphore_wait(go_sem, 1)
+        late_copies(start)
 
     level = level_of(deep - 1)
     for c in range(members):
@@ -1533,6 +1559,15 @@
             else:
                 result[part, 0:narrow] = value
 
+        if c == members - 3 and skewed:
+
+            @pl.when(jnp.logical_not(inner) & (core == 0))
+            def _():
+                nearest = jnp.where(has_up, up, down)
+                pl.semaphore_signal(
+                    go_sem, inc=1, device_id=(nearest, tp_c), device_id_type=MESH
+                )
+
         if c < members - 1:
             by_span(last_level)
             continue
@@ -1542,13 +1577,7 @@
                 last_level(pl.ds(first, rows // 2))
             send(level)
 
-    arrivals = out.at[:, pl.ds(0, (2 * members - 1) * narrow)]
-
-    def results(level, carry):
-        bulk(arrivals, result_sems.at[1, level]).wait_recv()
-        return carry
-
-    lax.fori_loop(0, deep, results, 0)
+    bulk(out.at[:, pl.ds(0, deep * (2 * members - 1) * narrow)], result_sems.at[1]).wait_recv()
 
     sends_done(w_out, 2, 1)
     for index, buffer, size in ((0, band, WINDOW), (2, pool_band, pool_pad)):
@@ -1561,12 +1590,9 @@
         def _(index=index, buffer=buffer, size=size):
             halo(index + 1, buffer, size, True).wait_send()
 
-    def results_sent(level, carry):
-        bulk(rounded.at[level, most(plane), :], result_sems.at[0, level]).wait_send()
-        result_own(level).wait()
-        return carry
-
-    lax.fori_loop(0, deep, results_sent, 0)
+    bulk(rounded.at[:, most(plane), :], result_sems.at[0]).wait_send()
+    here_rows = rounded.at[:, pl.ds(0, share), :]
+    pltpu.make_async_copy(here_rows, here_rows, result_sems.at[2]).wait()
 
 
 def plane_scratch(count, members, rows, features, depth, kw, qw, pw, width):
@@ -1611,13 +1637,14 @@
         dma((1,)),
         dma((3, tiles)),
         dma((3,)),
-        dma((3, 2 * tiles)),
+        dma((2, 2 * tiles)),
         dma((3,)),
-        dma((3, pooled_parts)),
+        dma((2, pooled_parts)),
         dma((3,)),
         dma((4,)),
         dma((4,)),
-        dma((3, deep)),
+        dma((3,)),
+        pltpu.SemaphoreType.REGULAR,
     ]
 
 

time: 151 us -> 149 us (0.987)
  Pallas kernels: 150 us -> 147 us
    pallas_call x1, Pallas kernels: 150 us -> 147 us  [shards(): pl.pallas_call(functools.partial(kernel, count, members), out_shape=resul...]
where the time goes in v6:
time: 149 us; the launch traced here: 148 us
  Pallas kernels  147 us (99%)
    pallas_call x1, Pallas kernels, shards(): pl.pallas_call(functools.partial(kernel, count, members), out_shape=resul...  147 us

profile of v6, /device:TPU:1, one launch (start us, length us, event | category | flops | bytes accessed | tf_op | source)
XLA Modules:
  0.0 148.2 jit_solution(3330363183753791981)
XLA Ops:
  0.0 147.0 %shard_map.145 = bf16[192,4096]{1,0:T(8,128)(2,1)S(1)} custom-call(bf16[768,1024]{1,0:T(8,128)(2,1)} %tokens.1, bf16[512,512]{1,0:T(8,128)(2,1)} %wq.1, bf16[512,256]{1,0:T(8,128)(2,1)} %wk.1, bf16[512,256]{1,0:T(8,128)(2,1)} %wv.1, bf16[512,256]{1,0:T(8,128)(2,1)} %wp.1, bf16[256,512]{1,0:T(8,128)(2,1)} %wop.1, bf16[512,512]{1,0:T(8,128)(2,1)} %woa.1, ...), custom_call_target="tpu_custom_call" | custom-call | tf_op jit(solution)/shard_map/pallas_call | solution.py:1750
  147.0 1.1 copy.17

commit v7 on v6

--- a/solution.py
+++ b/solution.py
@@ -1571,11 +1571,16 @@
         if c < members - 1:
             by_span(last_level)
             continue
-        for side, send in ((1 - x, send_far), (x, send_near)):
-            for start_row in range(0, rows, rows // 2):
-                first = pl.multiple_of(side * rows + start_row, rows // 2)
-                last_level(pl.ds(first, rows // 2))
-            send(level)
+        for side in (1 - x, x):
+            for chip in (1 - y, y):
+                first = (side * members + chip * 2) * share
+                last_level(pl.ds(pl.multiple_of(first, 2 * share), 2 * share))
+                if side is x and chip is y:
+                    result_copy(level, x, tp_c).start()
+                    result_own(level).start()
+                else:
+                    result_copy(level, side, chip * 2 + core).start()
+                    result_copy(level, side, chip * 2 + 1 - core).start()
 
     bulk(out.at[:, pl.ds(0, deep * (2 * members - 1) * narrow)], result_sems.at[1]).wait_recv()
 

time: 149 us -> 149 us (level)
  no operation moved by 1% of the time
where the time goes in v7:
time: 149 us; the launch traced here: 148 us
  Pallas kernels  147 us (99%)
    pallas_call x1, Pallas kernels, shards(): pl.pallas_call(functools.partial(kernel, count, members), out_shape=resul...  147 us

profile of v7, /device:TPU:1, one launch (start us, length us, event | category | flops | bytes accessed | tf_op | source)
XLA Modules:
  0.0 148.3 jit_solution(14480215077910982508)
XLA Ops:
  0.0 147.1 %shard_map.145 = bf16[192,4096]{1,0:T(8,128)(2,1)S(1)} custom-call(bf16[768,1024]{1,0:T(8,128)(2,1)} %tokens.1, bf16[512,512]{1,0:T(8,128)(2,1)} %wq.1, bf16[512,256]{1,0:T(8,128)(2,1)} %wk.1, bf16[512,256]{1,0:T(8,128)(2,1)} %wv.1, bf16[512,256]{1,0:T(8,128)(2,1)} %wp.1, bf16[256,512]{1,0:T(8,128)(2,1)} %wop.1, bf16[512,512]{1,0:T(8,128)(2,1)} %woa.1, ...), custom_call_target="tpu_custom_call" | custom-call | tf_op jit(solution)/shard_map/pallas_call | solution.py:1755
  147.1 1.1 copy.17
